TPU v7x, 32 devices: a whole 2x2x4 slice. The times are simulated.
32 devices in a mesh: tp: 32 (over z, y, x, core).
Axes of the slice: x: 2, y: 2, z: 4, core: 2. Of those that a mesh axis runs over, the one named last changes fastest.
Arguments:
- stream: bfloat16 [1024, 2048], P('tp'), may hold values from -15 to 15
- norm_gain: bfloat16 [4096], replicated, may hold values from 0.099609375 to 1.8984375
- query_weight: bfloat16 [65536, 128], P('tp'), may hold values from -0.09375 to 0.09375
- key_weight: bfloat16 [65536, 128], P('tp'), may hold values from -0.09375 to 0.09375
- value_weight: bfloat16 [65536, 128], P('tp'), may hold values from -0.09375 to 0.09375
- gate_weight: bfloat16 [65536, 128], P('tp'), may hold values from -0.09375 to 0.09375
- write_weight: bfloat16 [4096, 16], replicated, may hold values from -0.09375 to 0.09375
- decay_weight: bfloat16 [4096, 16], replicated, may hold values from -0.09375 to 0.09375
- decay_rate: float32 [16], replicated, may hold values from 0.02 to 2
- head_gain: bfloat16 [128], replicated, may hold values from 0.099609375 to 1.8984375
- out_weight: bfloat16 [65536, 128], P('tp'), may hold values from -0.125 to 0.125
- state: float32 [8192, 128, 128], P('tp'), may hold values from -4 to 4
Outputs:
- stream_out: bfloat16 [1024, 2048], P('tp')
- state_out: float32 [8192, 128, 128], P('tp')
All inputs are finite; a program needn't handle non-finite values.
Results may differ from a plain program's by a relative error of at most 0.012.
Values may be sent and summed in bfloat16 or wider, within the bound.
A program may use at most 128 MiB of HBM per device.

v0:
```python
import jax
import jax.numpy as jnp
from jax import lax
from jax.sharding import PartitionSpec as P

EPS = 1e-06


def from_partner(shard, axis, bit):
    return lax.ppermute(shard, axis, [(i, i ^ 1 << bit) for i in range(lax.axis_size(axis))])


def shortened(shard):

    def short(part):
        return part.astype(jnp.bfloat16) if part.dtype == jnp.float32 else part

    return jax.tree.map(short, shard)


def per_device(
    stream,
    norm_gain,
    query_weight,
    key_weight,
    value_weight,
    gate_weight,
    write_weight,
    decay_weight,
    decay_rate,
    head_gain,
    out_weight,
    state,
):
    highest = lax.Precision.HIGHEST
    devices = lax.axis_size("tp")
    my_index = lax.axis_index("tp")
    head_count = decay_rate.shape[0]
    head_size = head_gain.shape[0]
    group_count = devices // head_count
    head_bits = head_count.bit_length() - 1
    group_bits = group_count.bit_length() - 1
    my_head = my_index % head_count
    my_group = my_index // head_count
    own_rows, own_cols = stream.shape
    model_width = own_cols * group_count
    gathered = stream
    for bit_level in range(head_bits):
        partner = from_partner(gathered, "tp", bit_level)
        upper_bit = my_index // (1 << bit_level) % 2
        gathered = jnp.where(
            upper_bit == 1,
            jnp.concatenate([partner, gathered], 0),
            jnp.concatenate([gathered, partner], 0),
        )
    stream_f = gathered.astype(jnp.float32)
    gain_block = lax.dynamic_slice_in_dim(norm_gain, my_group * own_cols, own_cols, 0).astype(
        jnp.float32
    )
    gained = (stream_f * gain_block[None, :]).astype(jnp.bfloat16)
    squares = jnp.sum(stream_f * stream_f, axis=1)
    write_rows = lax.dynamic_slice(write_weight, (my_group * own_cols, my_head), (own_cols, 1))
    decay_rows = lax.dynamic_slice(decay_weight, (my_group * own_cols, my_head), (own_cols, 1))
    big_weights = jnp.concatenate([query_weight, key_weight, value_weight, gate_weight], axis=1)
    partial_value = jnp.dot(gained, big_weights, preferred_element_type=jnp.float32)
    small_part = jnp.dot(
        gained,
        jnp.concatenate([write_rows, decay_rows], axis=1),
        preferred_element_type=jnp.float32,
    )
    for step_index in range(group_bits):
        bit_level = head_bits + group_bits - 1 - step_index
        upper_bit = my_index // (1 << bit_level) % 2
        half_rows = partial_value.shape[0] // 2
        kept = [
            lax.dynamic_slice_in_dim(member, upper_bit * half_rows, half_rows, 0)
            for member in (partial_value, small_part, squares)
        ]
        sent = [
            lax.dynamic_slice_in_dim(member, (1 - upper_bit) * half_rows, half_rows, 0)
            for member in (partial_value, small_part, squares)
        ]
        received = from_partner(
            (shortened(sent[0]), shortened(sent[1]), shortened(sent[2])), "tp", bit_level
        )
        partial_value = kept[0] + received[0]
        small_part = kept[1] + received[1]
        squares = kept[2] + received[2]
    row_scale = lax.rsqrt(squares / model_width + EPS)
    projected = (partial_value * row_scale[:, None]).astype(jnp.bfloat16).astype(jnp.float32)
    small_pre = (small_part * row_scale[:, None]).astype(jnp.bfloat16).astype(jnp.float32)
    query_raw = projected[:, :head_size]
    key_raw = projected[:, head_size : 2 * head_size]
    value_vec = projected[:, 2 * head_size : 3 * head_size]
    gate_vec = projected[:, 3 * head_size :]
    query_vec = (
        query_raw
        * lax.rsqrt(jnp.sum(query_raw * query_raw, axis=-1, keepdims=True) + EPS)
        * head_size ** (-0.5)
    )
    key_vec = key_raw * lax.rsqrt(jnp.sum(key_raw * key_raw, axis=-1, keepdims=True) + EPS)
    strength = jax.nn.sigmoid(small_pre[:, 0])
    rate_value = lax.dynamic_slice_in_dim(decay_rate, my_head, 1, 0)[0]
    decay_factor = jnp.exp(-rate_value * jax.nn.softplus(small_pre[:, 1]))
    recalled = jnp.einsum("bdj,bd->bj", state, key_vec, precision=highest)
    correction = strength[:, None] * (value_vec - decay_factor[:, None] * recalled)
    updated = decay_factor[:, None, None] * state + key_vec[:, :, None] * correction[:, None, :]
    readout = jnp.einsum("bdj,bd->bj", updated, query_vec, precision=highest)
    scaling = lax.rsqrt(jnp.mean(readout * readout, axis=1) + EPS)
    gated = (readout * head_gain.astype(jnp.float32)[None, :] * jax.nn.silu(gate_vec)).astype(
        jnp.bfloat16
    )
    all_gated = gated
    all_scaling = scaling
    for step_index in range(group_bits):
        bit_level = head_bits + step_index
        upper_bit = my_index // (1 << bit_level) % 2
        other_gated, other_scaling = (
            from_partner(all_gated, "tp", bit_level),
            from_partner(all_scaling.astype(jnp.bfloat16), "tp", bit_level).astype(
                all_scaling.dtype
            ),
        )
        all_gated = jnp.where(
            upper_bit == 1,
            jnp.concatenate([other_gated, all_gated], 0),
            jnp.concatenate([all_gated, other_gated], 0),
        )
        all_scaling = jnp.where(
            upper_bit == 1,
            jnp.concatenate([other_scaling, all_scaling], 0),
            jnp.concatenate([all_scaling, other_scaling], 0),
        )
    head_sums = (
        lax.dot_general(
            all_gated, out_weight, (((1,), (1,)), ((), ())), preferred_element_type=jnp.float32
        )
        * all_scaling[:, None]
    )
    for step_index in range(head_bits):
        bit_level = head_bits - 1 - step_index
        upper_bit = my_index // (1 << bit_level) % 2
        half_rows = head_sums.shape[0] // 2
        kept_sums = lax.dynamic_slice_in_dim(head_sums, upper_bit * half_rows, half_rows, 0)
        sent_sums = lax.dynamic_slice_in_dim(head_sums, (1 - upper_bit) * half_rows, half_rows, 0)
        head_sums = kept_sums + from_partner(
            sent_sums.astype(jnp.bfloat16), "tp", bit_level
        ).astype(sent_sums.dtype)
    result = (stream.astype(jnp.float32) + head_sums).astype(jnp.bfloat16)
    return (result, updated)


def solution(mesh):
    placed = (
        P("tp", None),
        P(),
        P("tp", None),
        P("tp", None),
        P("tp", None),
        P("tp", None),
        P(),
        P(),
        P(),
        P(),
        P("tp", None),
        P("tp", None, None),
    )
    return jax.shard_map(
        per_device,
        mesh=mesh,
        in_specs=placed,
        out_specs=(P("tp", None), P("tp", None, None)),
        check_vma=False,
    )
```

profile of v0, /device:TPU:0, one launch (start us, length us, event | category | flops | bytes accessed | tf_op | source)
XLA Modules:
  0.0 162.3 jit_solution(7793796808106050934)
XLA Ops:
  1.2 1.2 collective-permute-done
  2.4 1.0 maximum_select_fusion.3
  3.4 2.9 %collective-permute-start.1 = (bf16[64,2048]{1,0:T(8,128)(2,1)S(1)}, bf16[64,2048]{1,0:T(8,128)(2,1)S(1)}, u32[]{:S(2)}, u32[]{:S(2)}) collective-permute-start(bf16[64,2048]{1,0:T(8,128)(2,1)S(1)} %maximum_select_fusion.3), channel_id=1, source_target_pairs={{0,2},{1,3},{2,0},{3,1},{4,6},{5,7},{6,4},{7,5},{8,10},{9,11},{10,... | collective-permute-start | bytes 786440 | tf_op jit(solution)/shard_map/ppermute | solution.py:10
  6.3 6.6 %collective-permute-done.1 = bf16[64,2048]{1,0:T(8,128)(2,1)S(1)} collective-permute-done((bf16[64,2048]{1,0:T(8,128)(2,1)S(1)}, bf16[64,2048]{1,0:T(8,128)(2,1)S(1)}, u32[]{:S(2)}, u32[]{:S(2)}) %collective-permute-start.1) | collective-permute-done | bytes 262176 | tf_op jit(solution)/shard_map/ppermute | solution.py:10
  13.1 1.8 %collective-permute-start.2 = (bf16[128,2048]{1,0:T(8,128)(2,1)S(1)}, bf16[128,2048]{1,0:T(8,128)(2,1)S(1)}, u32[]{:S(2)}, u32[]{:S(2)}) collective-permute-start(bf16[128,2048]{1,0:T(8,128)(2,1)S(1)} %maximum_select_fusion.2), channel_id=1, source_target_pairs={{0,4},{1,5},{2,6},{3,7},{4,0},{5,1},{6,2},{7,3},{8,12},{9,13},{10,... | collective-permute-start | bytes 1572872 | tf_op jit(solution)/shard_map/ppermute | solution.py:10
  14.9 11.6 %collective-permute-done.2 = bf16[128,2048]{1,0:T(8,128)(2,1)S(1)} collective-permute-done((bf16[128,2048]{1,0:T(8,128)(2,1)S(1)}, bf16[128,2048]{1,0:T(8,128)(2,1)S(1)}, u32[]{:S(2)}, u32[]{:S(2)}) %collective-permute-start.2) | collective-permute-done | bytes 524320 | tf_op jit(solution)/shard_map/ppermute | solution.py:10
  26.8 1.6 collective-permute-start.3
  30.1 1.2 dynamic_slice.54
  33.4 17.3 %collective-permute-done.3 = bf16[256,2048]{1,0:T(8,128)(2,1)S(1)} collective-permute-done((bf16[256,2048]{1,0:T(8,128)(2,1)S(1)}, bf16[256,2048]{1,0:T(8,128)(2,1)S(1)}, u32[]{:S(2)}, u32[]{:S(2)}) %collective-permute-start.3) | collective-permute-done | bytes 1048608 | tf_op jit(solution)/shard_map/ppermute | solution.py:10
  51.3 2.3 %collective-permute-start.4 = (bf16[256,2]{0,1:T(2,128)(2,1)S(1)}, bf16[256,2]{0,1:T(2,128)(2,1)S(1)}, u32[]{:S(2)}, u32[]{:S(2)}) collective-permute-start(bf16[256,2]{0,1:T(2,128)(2,1)S(1)} %fusion.27), channel_id=1, source_target_pairs={{0,16},{1,17},{2,18},{3,19},{4,20},{5,21},{6,22},{7,23},{8,24},{9,... | collective-permute-start | bytes 3080 | tf_op jit(solution)/shard_map/ppermute | solution.py:10
  55.1 1.3 fusion.2
  56.4 2.3 %collective-permute-start.6 = (bf16[256,512]{1,0:T(8,128)(2,1)S(1)}, bf16[256,512]{1,0:T(8,128)(2,1)S(1)}, u32[]{:S(2)}, u32[]{:S(2)}) collective-permute-start(bf16[256,512]{1,0:T(8,128)(2,1)S(1)} %dynamic-slice_convert_fusion.3), channel_id=1, source_target_pairs={{0,16},{1,17},{2,18},{3,19},{4,20},{5,21},{6,22},{7,23},{8,24},{9,... | collective-permute-start | bytes 786440 | tf_op jit(solution)/shard_map/ppermute | solution.py:10
  58.8 1.9 %collective-permute-done.5 = bf16[256]{0:T(256)(128)(2,1)S(1)} collective-permute-done((bf16[256]{0:T(256)(128)(2,1)S(1)}, bf16[256]{0:T(256)(128)(2,1)S(1)}, u32[]{:S(2)}, u32[]{:S(2)}) %collective-permute-start.5) | collective-permute-done | bytes 544 | tf_op jit(solution)/shard_map/ppermute | solution.py:10
  60.8 7.7 %collective-permute-done.6 = bf16[256,512]{1,0:T(8,128)(2,1)S(1)} collective-permute-done((bf16[256,512]{1,0:T(8,128)(2,1)S(1)}, bf16[256,512]{1,0:T(8,128)(2,1)S(1)}, u32[]{:S(2)}, u32[]{:S(2)}) %collective-permute-start.6) | collective-permute-done | bytes 262176 | tf_op jit(solution)/shard_map/ppermute | solution.py:10
  69.0 14.7 %fusion.41 = f32[256,1,128]{2,1,0:T(1,128)S(1)} fusion(f32[256,128,1]{1,2,0:T(1,128)S(1)} %bitcast.21, f32[256,128,128]{2,1,0:T(8,128)S(1)} %bitcast.20), kind=kOutput, calls=%fused_computation.77 | convolution fusion | flops 50331648 | bytes 17039360 | tf_op jit(solution)/shard_map/bdj,bd->bj/dot_general | solution.py:105
  83.9 6.1 %multiply_add_fusion = f32[256,128,128]{2,1,0:T(8,128)S(1)} fusion(f32[256,128,128]{2,1,0:T(8,128)S(1)} %bitcast.20, f32[256,128]{1,0:T(8,128)S(1)} %get-tuple-element.5, f32[256,128]{1,0:T(8,128)S(1)} %slice_multiply_fusion, f32[256]{0:T(256)S(1)} %fusion.30), kind=kLoop, calls=%fused_computation | loop fusion | flops 12582912 | bytes 33817600 | tf_op jit(solution)/shard_map/add | solution.py:107
  90.0 14.5 %fusion.42 = f32[256,1,128]{2,1,0:T(1,128)S(1)} fusion(f32[256,128,128]{2,1,0:T(8,128)S(1)} %multiply_add_fusion, f32[256,128,1]{1,2,0:T(1,128)S(1)} %bitcast.22), kind=kOutput, calls=%fused_computation.78 | convolution fusion | flops 50331648 | bytes 17039360 | tf_op jit(solution)/shard_map/bdj,bd->bj/dot_general | solution.py:108
  104.8 2.9 %collective-permute-start.7 = (bf16[256,128]{1,0:T(8,128)(2,1)S(1)}, bf16[256,128]{1,0:T(8,128)(2,1)S(1)}, u32[]{:S(2)}, u32[]{:S(2)}) collective-permute-start(bf16[256,128]{1,0:T(8,128)(2,1)S(1)} %get-tuple-element.6), channel_id=1, source_target_pairs={{0,16},{1,17},{2,18},{3,19},{4,20},{5,21},{6,22},{7,23},{8,24},{9,... | collective-permute-start | bytes 196616 | tf_op jit(solution)/shard_map/ppermute | solution.py:10
  107.7 1.5 collective-permute-done.8
  109.2 1.5 collective-permute-done.7
  111.4 1.9 %copy-done.2 = f32[512,2048]{1,0:T(8,128)} copy-done((f32[512,2048]{1,0:T(8,128)}, f32[512,2048]{1,0:T(8,128)S(1)}, u32[]{:S(2)}) %copy-start.2) | copy-done | bytes 4194328
  113.5 2.7 %collective-permute-start.9 = (bf16[256,2048]{1,0:T(8,128)(2,1)S(1)}, bf16[256,2048]{1,0:T(8,128)(2,1)}, u32[]{:S(2)}, u32[]{:S(2)}) collective-permute-start(bf16[256,2048]{1,0:T(8,128)(2,1)S(1)} %dynamic-slice_convert_fusion), channel_id=1, source_target_pairs={{0,8},{1,9},{2,10},{3,11},{4,12},{5,13},{6,14},{7,15},{8,0},{9,1},... | collective-permute-start | bytes 3145736 | tf_op jit(solution)/shard_map/ppermute | solution.py:10
  116.2 21.0 %collective-permute-done.9 = bf16[256,2048]{1,0:T(8,128)(2,1)} collective-permute-done((bf16[256,2048]{1,0:T(8,128)(2,1)S(1)}, bf16[256,2048]{1,0:T(8,128)(2,1)}, u32[]{:S(2)}, u32[]{:S(2)}) %collective-permute-start.9) | collective-permute-done | bytes 1048608 | tf_op jit(solution)/shard_map/ppermute | solution.py:10
  137.2 2.2 %convert_add_fusion = f32[256,2048]{1,0:T(8,128)S(1)} fusion(bf16[256,2048]{1,0:T(8,128)(2,1)} %collective-permute-done.9, f32[512,2048]{1,0:T(8,128)} %copy-done.2, s32[]{:T(128)S(6)} %select_n.192), kind=kLoop, calls=%fused_computation.15 | loop fusion | flops 1048576 | bytes 5242884 | tf_op jit(solution)/shard_map/add | solution.py:146
  139.5 1.5 collective-permute-start.10
  141.0 9.5 %collective-permute-done.10 = bf16[128,2048]{1,0:T(8,128)(2,1)} collective-permute-done((bf16[128,2048]{1,0:T(8,128)(2,1)S(1)}, bf16[128,2048]{1,0:T(8,128)(2,1)}, u32[]{:S(2)}, u32[]{:S(2)}) %collective-permute-start.10) | collective-permute-done | bytes 524320 | tf_op jit(solution)/shard_map/ppermute | solution.py:10
  150.5 1.1 convert_add_fusion.1
  151.6 1.0 copy-done.3
  152.6 1.4 collective-permute-start.11
  154.0 5.1 %collective-permute-done.11 = bf16[64,2048]{1,0:T(8,128)(2,1)S(1)} collective-permute-done((bf16[64,2048]{1,0:T(8,128)(2,1)S(1)}, bf16[64,2048]{1,0:T(8,128)(2,1)S(1)}, u32[]{:S(2)}, u32[]{:S(2)}) %collective-permute-start.11) | collective-permute-done | bytes 262176 | tf_op jit(solution)/shard_map/ppermute | solution.py:10
  159.1 1.1 convert_add_fusion.2
  160.3 1.3 collective-permute-done.12
  (60 shorter events, 8.8 us)
Async XLA Ops:
  0.6 110.1 %copy-start = (bf16[2048,128]{1,0:T(8,128)(2,1)S(1)}, bf16[2048,128]{1,0:T(8,128)(2,1)}, u32[]{:S(2)}) copy-start(bf16[2048,128]{1,0:T(8,128)(2,1)} %param.22) | copy-start | bytes 1572868
  0.6 1.8 %collective-permute-start = (bf16[32,2048]{1,0:T(8,128)(2,1)}, bf16[32,2048]{1,0:T(8,128)(2,1)S(1)}, u32[]{:S(2)}, u32[]{:S(2)}) collective-permute-start(bf16[32,2048]{1,0:T(8,128)(2,1)} %param.12), channel_id=1, source_target_pairs={{0,1},{1,0},{2,3},{3,2},{4,5},{5,4},{6,7},{7,6},{8,9},{9,8},{10,11... | collective-permute-start | bytes 393224 | tf_op jit(solution)/shard_map/ppermute | solution.py:10
  3.4 9.5 %collective-permute-start.1 = (bf16[64,2048]{1,0:T(8,128)(2,1)S(1)}, bf16[64,2048]{1,0:T(8,128)(2,1)S(1)}, u32[]{:S(2)}, u32[]{:S(2)}) collective-permute-start(bf16[64,2048]{1,0:T(8,128)(2,1)S(1)} %maximum_select_fusion.3), channel_id=1, source_target_pairs={{0,2},{1,3},{2,0},{3,1},{4,6},{5,7},{6,4},{7,5},{8,10},{9,11},{10,... | collective-permute-start | bytes 786440 | tf_op jit(solution)/shard_map/ppermute | solution.py:10
  13.1 13.5 %collective-permute-start.2 = (bf16[128,2048]{1,0:T(8,128)(2,1)S(1)}, bf16[128,2048]{1,0:T(8,128)(2,1)S(1)}, u32[]{:S(2)}, u32[]{:S(2)}) collective-permute-start(bf16[128,2048]{1,0:T(8,128)(2,1)S(1)} %maximum_select_fusion.2), channel_id=1, source_target_pairs={{0,4},{1,5},{2,6},{3,7},{4,0},{5,1},{6,2},{7,3},{8,12},{9,13},{10,... | collective-permute-start | bytes 1572872 | tf_op jit(solution)/shard_map/ppermute | solution.py:10
  26.8 23.8 %collective-permute-start.3 = (bf16[256,2048]{1,0:T(8,128)(2,1)S(1)}, bf16[256,2048]{1,0:T(8,128)(2,1)S(1)}, u32[]{:S(2)}, u32[]{:S(2)}) collective-permute-start(bf16[256,2048]{1,0:T(8,128)(2,1)S(1)} %maximum_select_fusion.1), channel_id=1, source_target_pairs={{0,8},{1,9},{2,10},{3,11},{4,12},{5,13},{6,14},{7,15},{8,0},{9,1},... | collective-permute-start | bytes 3145736 | tf_op jit(solution)/shard_map/ppermute | solution.py:10
  33.3 21.8 %copy-start.5 = (bf16[2048,128]{1,0:T(8,128)(2,1)S(1)}, bf16[2048,128]{1,0:T(8,128)(2,1)}, u32[]{:S(2)}) copy-start(bf16[2048,128]{1,0:T(8,128)(2,1)} %param.17) | copy-start | bytes 1572868
  33.3 21.8 %copy-start.6 = (bf16[2048,128]{1,0:T(8,128)(2,1)S(1)}, bf16[2048,128]{1,0:T(8,128)(2,1)}, u32[]{:S(2)}) copy-start(bf16[2048,128]{1,0:T(8,128)(2,1)} %param.16) | copy-start | bytes 1572868
  33.3 21.8 %copy-start.7 = (bf16[2048,128]{1,0:T(8,128)(2,1)S(1)}, bf16[2048,128]{1,0:T(8,128)(2,1)}, u32[]{:S(2)}) copy-start(bf16[2048,128]{1,0:T(8,128)(2,1)} %param.15) | copy-start | bytes 1572868
  33.4 21.8 %copy-start.8 = (bf16[2048,128]{1,0:T(8,128)(2,1)S(1)}, bf16[2048,128]{1,0:T(8,128)(2,1)}, u32[]{:S(2)}) copy-start(bf16[2048,128]{1,0:T(8,128)(2,1)} %param.14) | copy-start | bytes 1572868
  50.6 18.3 %slice-start = ((s8[16777216]{0:T(1024)(128)(4,1)}), s8[4194304]{0:T(1024)(128)(4,1)S(1)}, s32[]{:S(2)}) async-start(s8[16777216]{0:T(1024)(128)(4,1)} %bitcast.19), calls=%async_computation | async-start | bytes 8388608
  50.6 18.3 %slice-start.1 = ((s8[16777216]{0:T(1024)(128)(4,1)}), s8[4194304]{0:T(1024)(128)(4,1)S(1)}, s32[]{:S(2)}) async-start(s8[16777216]{0:T(1024)(128)(4,1)} %bitcast.19), calls=%async_computation.1 | async-start | bytes 8388608
  51.3 9.4 %collective-permute-start.4 = (bf16[256,2]{0,1:T(2,128)(2,1)S(1)}, bf16[256,2]{0,1:T(2,128)(2,1)S(1)}, u32[]{:S(2)}, u32[]{:S(2)}) collective-permute-start(bf16[256,2]{0,1:T(2,128)(2,1)S(1)} %fusion.27), channel_id=1, source_target_pairs={{0,16},{1,17},{2,18},{3,19},{4,20},{5,21},{6,22},{7,23},{8,24},{9,... | collective-permute-start | bytes 3080 | tf_op jit(solution)/shard_map/ppermute | solution.py:10
  54.4 14.5 %slice-start.2 = ((s8[16777216]{0:T(1024)(128)(4,1)}), s8[4194304]{0:T(1024)(128)(4,1)S(1)}, s32[]{:S(2)}) async-start(s8[16777216]{0:T(1024)(128)(4,1)} %bitcast.19), calls=%async_computation.2 | async-start | bytes 8388608
  54.4 14.5 %slice-start.3 = ((s8[16777216]{0:T(1024)(128)(4,1)}), s8[4194304]{0:T(1024)(128)(4,1)S(1)}, s32[]{:S(2)}) async-start(s8[16777216]{0:T(1024)(128)(4,1)} %bitcast.19), calls=%async_computation.3 | async-start | bytes 8388608
  54.4 6.2 %collective-permute-start.5 = (bf16[256]{0:T(256)(128)(2,1)S(1)}, bf16[256]{0:T(256)(128)(2,1)S(1)}, u32[]{:S(2)}, u32[]{:S(2)}) collective-permute-start(bf16[256]{0:T(256)(128)(2,1)S(1)} %dynamic_slice.99), channel_id=1, source_target_pairs={{0,16},{1,17},{2,18},{3,19},{4,20},{5,21},{6,22},{7,23},{8,24},{9,... | collective-permute-start | bytes 1544 | tf_op jit(solution)/shard_map/ppermute | solution.py:10
  56.4 12.1 %collective-permute-start.6 = (bf16[256,512]{1,0:T(8,128)(2,1)S(1)}, bf16[256,512]{1,0:T(8,128)(2,1)S(1)}, u32[]{:S(2)}, u32[]{:S(2)}) collective-permute-start(bf16[256,512]{1,0:T(8,128)(2,1)S(1)} %dynamic-slice_convert_fusion.3), channel_id=1, source_target_pairs={{0,16},{1,17},{2,18},{3,19},{4,20},{5,21},{6,22},{7,23},{8,24},{9,... | collective-permute-start | bytes 786440 | tf_op jit(solution)/shard_map/ppermute | solution.py:10
  90.0 14.6 %copy-start.1 = (f32[256,128,128]{2,1,0:T(8,128)}, f32[256,128,128]{2,1,0:T(8,128)S(1)}, u32[]{:S(2)}) copy-start(f32[256,128,128]{2,1,0:T(8,128)S(1)} %multiply_add_fusion) | copy-start | bytes 50331652
  104.7 4.5 %collective-permute-start.8 = (bf16[256]{0:T(256)(128)(2,1)S(1)}, bf16[256]{0:T(256)(128)(2,1)S(1)}, u32[]{:S(2)}, u32[]{:S(2)}) collective-permute-start(bf16[256]{0:T(256)(128)(2,1)S(1)} %get-tuple-element.11), channel_id=1, source_target_pairs={{0,16},{1,17},{2,18},{3,19},{4,20},{5,21},{6,22},{7,23},{8,24},{9,... | collective-permute-start | bytes 1544 | tf_op jit(solution)/shard_map/ppermute | solution.py:10
  104.8 5.9 %collective-permute-start.7 = (bf16[256,128]{1,0:T(8,128)(2,1)S(1)}, bf16[256,128]{1,0:T(8,128)(2,1)S(1)}, u32[]{:S(2)}, u32[]{:S(2)}) collective-permute-start(bf16[256,128]{1,0:T(8,128)(2,1)S(1)} %get-tuple-element.6), channel_id=1, source_target_pairs={{0,16},{1,17},{2,18},{3,19},{4,20},{5,21},{6,22},{7,23},{8,24},{9,... | collective-permute-start | bytes 196616 | tf_op jit(solution)/shard_map/ppermute | solution.py:10
  111.4 1.9 %copy-start.2 = (f32[512,2048]{1,0:T(8,128)}, f32[512,2048]{1,0:T(8,128)S(1)}, u32[]{:S(2)}) copy-start(f32[512,2048]{1,0:T(8,128)S(1)} %convolution_multiply_fusion) | copy-start | bytes 12582916
  113.5 23.7 %collective-permute-start.9 = (bf16[256,2048]{1,0:T(8,128)(2,1)S(1)}, bf16[256,2048]{1,0:T(8,128)(2,1)}, u32[]{:S(2)}, u32[]{:S(2)}) collective-permute-start(bf16[256,2048]{1,0:T(8,128)(2,1)S(1)} %dynamic-slice_convert_fusion), channel_id=1, source_target_pairs={{0,8},{1,9},{2,10},{3,11},{4,12},{5,13},{6,14},{7,15},{8,0},{9,1},... | collective-permute-start | bytes 3145736 | tf_op jit(solution)/shard_map/ppermute | solution.py:10
  139.4 22.2 %copy-start.4 = (bf16[32,2048]{1,0:T(8,128)(2,1)S(1)}, bf16[32,2048]{1,0:T(8,128)(2,1)}, u32[]{:S(2)}) copy-start(bf16[32,2048]{1,0:T(8,128)(2,1)} %param.12) | copy-start | bytes 393220
  139.5 11.0 %collective-permute-start.10 = (bf16[128,2048]{1,0:T(8,128)(2,1)S(1)}, bf16[128,2048]{1,0:T(8,128)(2,1)}, u32[]{:S(2)}, u32[]{:S(2)}) collective-permute-start(bf16[128,2048]{1,0:T(8,128)(2,1)S(1)} %dynamic-slice_convert_fusion.1), channel_id=1, source_target_pairs={{0,4},{1,5},{2,6},{3,7},{4,0},{5,1},{6,2},{7,3},{8,12},{9,13},{10,... | collective-permute-start | bytes 1572872 | tf_op jit(solution)/shard_map/ppermute | solution.py:10
  151.6 1.0 copy-start.3
  152.6 6.4 %collective-permute-start.11 = (bf16[64,2048]{1,0:T(8,128)(2,1)S(1)}, bf16[64,2048]{1,0:T(8,128)(2,1)S(1)}, u32[]{:S(2)}, u32[]{:S(2)}) collective-permute-start(bf16[64,2048]{1,0:T(8,128)(2,1)S(1)} %dynamic-slice_convert_fusion.2), channel_id=1, source_target_pairs={{0,2},{1,3},{2,0},{3,1},{4,6},{5,7},{6,4},{7,5},{8,10},{9,11},{10,... | collective-permute-start | bytes 786440 | tf_op jit(solution)/shard_map/ppermute | solution.py:10
  160.2 1.4 collective-permute-start.12
where the time goes:
time: 163 us; the launch traced here: 162 us
  waiting for transfers between devices  86.2 us (53%)
  matrix products  31.9 us (20%)
  starting transfers between devices  20.9 us (13%)
  other arithmetic  15.5 us (10%)
  local copies, waits for them, and re-layouts  6.29 us (4%)
    ppermute x13, waiting for transfers between devices, from_partner(): lax.ppermute(shard, axis, [(i, i ^ 1 << bit) for i in range(lax.axis_size...  86.2 us
    ppermute x13, starting transfers between devices, from_partner(): lax.ppermute(shard, axis, [(i, i ^ 1 << bit) for i in range(lax.axis_size...  20.9 us
    dot_general x1, matrix products, per_device(): recalled = jnp.einsum('bdj,bd->bj', state, key_vec, precision=highest)  14.7 us
    dot_general x1, matrix products, per_device(): readout = jnp.einsum('bdj,bd->bj', updated, query_vec, precision=highest)  14.5 us
    add x1, other arithmetic, per_device(): decay_factor[:, None, None] * state  6.11 us
    add x3, other arithmetic, per_device(): kept_sums + from_partner(sent_sums.astype(jnp.bfloat16), 'tp', bit_level)...  4.4 us
  transfers between devices with their start and end apart: 13, of which 12 were waited for; matrix products, arithmetic and copies ran while one was open for 4% of the time, Pallas kernels for 0%

commit v1 on v0

--- a/solution.py
+++ b/solution.py
@@ -1,6 +1,8 @@
 import jax
 import jax.numpy as jnp
 from jax import lax
+from jax.experimental import pallas as pl
+from jax.experimental.pallas import tpu as pltpu
 from jax.sharding import PartitionSpec as P
 
 EPS = 1e-06
@@ -16,6 +18,55 @@
         return part.astype(jnp.bfloat16) if part.dtype == jnp.float32 else part
 
     return jax.tree.map(short, shard)
+
+
+def state_kernel(state_ref, key_ref, query_ref, value_ref, rows_ref, new_ref, read_ref):
+    count = state_ref.shape[0]
+    for b in range(count):
+        memory = state_ref[b]
+        key = jnp.broadcast_to(key_ref[0, :, b : b + 1], memory.shape)
+        query = jnp.broadcast_to(query_ref[0, :, b : b + 1], memory.shape)
+        recalled = jnp.sum(memory * key, axis=0, keepdims=True)
+        asked = jnp.sum(memory * query, axis=0, keepdims=True)
+        strength = rows_ref[0, b : b + 1, :]
+        factor = rows_ref[1, b : b + 1, :]
+        overlap = rows_ref[2, b : b + 1, :]
+        change = strength * (value_ref[b : b + 1, :] - factor * recalled)
+        read_ref[b : b + 1, :] = factor * asked + overlap * change
+        new_ref[b] = factor * memory + key * change
+
+
+def state_step(state, query, key, value, strength, factor):
+    count, size, _ = state.shape
+    block = min(16, count)
+    steps = count // block
+    overlap = jnp.sum(query * key, axis=1)
+    rows = jnp.stack(
+        [jnp.broadcast_to(m[:, None], (count, size)) for m in (strength, factor, overlap)]
+    )
+
+    def columns(vec):
+        return vec.reshape(steps, block, size).transpose(0, 2, 1)
+
+    return pl.pallas_call(
+        state_kernel,
+        grid=(steps,),
+        in_specs=[
+            pl.BlockSpec((block, size, size), lambda i: (i, 0, 0)),
+            pl.BlockSpec((1, size, block), lambda i: (i, 0, 0)),
+            pl.BlockSpec((1, size, block), lambda i: (i, 0, 0)),
+            pl.BlockSpec((block, size), lambda i: (i, 0)),
+            pl.BlockSpec((3, block, size), lambda i: (0, i, 0)),
+        ],
+        out_specs=[
+            pl.BlockSpec((block, size, size), lambda i: (i, 0, 0)),
+            pl.BlockSpec((block, size), lambda i: (i, 0)),
+        ],
+        out_shape=[
+            jax.ShapeDtypeStruct(state.shape, state.dtype),
+            jax.ShapeDtypeStruct((count, size), jnp.float32),
+        ],
+    )(state, columns(key), columns(query), value, rows)
 
 
 def per_device(
@@ -32,7 +83,6 @@
     out_weight,
     state,
 ):
-    highest = lax.Precision.HIGHEST
     devices = lax.axis_size("tp")
     my_index = lax.axis_index("tp")
     head_count = decay_rate.shape[0]
@@ -102,10 +152,7 @@
     strength = jax.nn.sigmoid(small_pre[:, 0])
     rate_value = lax.dynamic_slice_in_dim(decay_rate, my_head, 1, 0)[0]
     decay_factor = jnp.exp(-rate_value * jax.nn.softplus(small_pre[:, 1]))
-    recalled = jnp.einsum("bdj,bd->bj", state, key_vec, precision=highest)
-    correction = strength[:, None] * (value_vec - decay_factor[:, None] * recalled)
-    updated = decay_factor[:, None, None] * state + key_vec[:, :, None] * correction[:, None, :]
-    readout = jnp.einsum("bdj,bd->bj", updated, query_vec, precision=highest)
+    updated, readout = state_step(state, query_vec, key_vec, value_vec, strength, decay_factor)
     scaling = lax.rsqrt(jnp.mean(readout * readout, axis=1) + EPS)
     gated = (readout * head_gain.astype(jnp.float32)[None, :] * jax.nn.silu(gate_vec)).astype(
         jnp.bfloat16

time: 163 us -> 153 us (0.939)
  matrix products: 31.9 us -> 2.66 us
  Pallas kernels: 0 us -> 20.3 us
  other arithmetic: 15.5 us -> 10.2 us
  local copies, waits for them, and re-layouts: 6.29 us -> 8.56 us
  waiting for transfers between devices: 86.2 us -> 88.3 us
    dot_general x2 -> x0, matrix products: 29.2 us -> none  [the longest x1 14.7 us: per_device(): recalled = jnp.einsum('bdj,bd->bj', state, key_vec, precision=highest)]
    pallas_call x0 -> x1, Pallas kernels: none -> 20.3 us  [state_step(): pl.pallas_call(state_kernel, grid=(steps,), in_specs=[pl.BlockSpec((block...]
    add x1 -> x0, other arithmetic: 6.11 us -> none  [per_device(): decay_factor[:, None, None] * state]
    reshape x0 -> x2, local copies, waits for them, and re-layouts: none -> 2.65 us  [columns(): return vec.reshape(steps, block, size).transpose(0, 2, 1)]
    ppermute x13, waiting for transfers between devices: 86.2 us -> 88.3 us  [from_partner(): lax.ppermute(shard, axis, [(i, i ^ 1 << bit) for i in range(lax.axis_size...]
  transfers between devices with their start and end apart: 13 -> 13, of which waited for: 12 -> 12; matrix products, arithmetic and copies ran while one was open for 4% -> 3% of each run, Pallas kernels for 0% -> 0%
where the time goes in v1:
time: 153 us; the launch traced here: 152 us
  waiting for transfers between devices  88.3 us (58%)
  starting transfers between devices  20.8 us (14%)
  Pallas kernels  20.3 us (13%)
  other arithmetic  10.2 us (7%)
  local copies, waits for them, and re-layouts  8.56 us (6%)
  matrix products  2.66 us (2%)
  between operations  1.6 us (1%)
    ppermute x13, waiting for transfers between devices, from_partner(): lax.ppermute(shard, axis, [(i, i ^ 1 << bit) for i in range(lax.axis_size...  88.3 us
    ppermute x13, starting transfers between devices, from_partner(): lax.ppermute(shard, axis, [(i, i ^ 1 << bit) for i in range(lax.axis_size...  20.8 us
    pallas_call x1, Pallas kernels, state_step(): pl.pallas_call(state_kernel, grid=(steps,), in_specs=[pl.BlockSpec((block...  20.3 us
    add x3, other arithmetic, per_device(): kept_sums + from_partner(sent_sums.astype(jnp.bfloat16), 'tp', bit_level)...  4.4 us
  transfers between devices with their start and end apart: 13, of which 12 were waited for; matrix products, arithmetic and copies ran while one was open for 3% of the time, Pallas kernels for 0%

profile of v1, /device:TPU:0, one launch (start us, length us, event | category | flops | bytes accessed | tf_op | source)
XLA Modules:
  0.0 152.5 jit_solution(1581067994810520369)
XLA Ops:
  1.2 1.2 collective-permute-done
  2.4 1.0 maximum_select_fusion.3
  3.5 2.9 %collective-permute-start.1 = (bf16[64,2048]{1,0:T(8,128)(2,1)S(1)}, bf16[64,2048]{1,0:T(8,128)(2,1)S(1)}, u32[]{:S(2)}, u32[]{:S(2)}) collective-permute-start(bf16[64,2048]{1,0:T(8,128)(2,1)S(1)} %maximum_select_fusion.3), channel_id=1, source_target_pairs={{0,2},{1,3},{2,0},{3,1},{4,6},{5,7},{6,4},{7,5},{8,10},{9,11},{10,... | collective-permute-start | bytes 786440 | tf_op jit(solution)/shard_map/ppermute | solution.py:12
  6.4 6.6 %collective-permute-done.1 = bf16[64,2048]{1,0:T(8,128)(2,1)S(1)} collective-permute-done((bf16[64,2048]{1,0:T(8,128)(2,1)S(1)}, bf16[64,2048]{1,0:T(8,128)(2,1)S(1)}, u32[]{:S(2)}, u32[]{:S(2)}) %collective-permute-start.1) | collective-permute-done | bytes 262176 | tf_op jit(solution)/shard_map/ppermute | solution.py:12
  13.1 1.8 %collective-permute-start.2 = (bf16[128,2048]{1,0:T(8,128)(2,1)S(1)}, bf16[128,2048]{1,0:T(8,128)(2,1)S(1)}, u32[]{:S(2)}, u32[]{:S(2)}) collective-permute-start(bf16[128,2048]{1,0:T(8,128)(2,1)S(1)} %maximum_select_fusion.2), channel_id=1, source_target_pairs={{0,4},{1,5},{2,6},{3,7},{4,0},{5,1},{6,2},{7,3},{8,12},{9,13},{10,... | collective-permute-start | bytes 1572872 | tf_op jit(solution)/shard_map/ppermute | solution.py:12
  14.9 11.6 %collective-permute-done.2 = bf16[128,2048]{1,0:T(8,128)(2,1)S(1)} collective-permute-done((bf16[128,2048]{1,0:T(8,128)(2,1)S(1)}, bf16[128,2048]{1,0:T(8,128)(2,1)S(1)}, u32[]{:S(2)}, u32[]{:S(2)}) %collective-permute-start.2) | collective-permute-done | bytes 524320 | tf_op jit(solution)/shard_map/ppermute | solution.py:12
  26.8 1.6 %collective-permute-start.3 = (bf16[256,2048]{1,0:T(8,128)(2,1)S(1)}, bf16[256,2048]{1,0:T(8,128)(2,1)S(1)}, u32[]{:S(2)}, u32[]{:S(2)}) collective-permute-start(bf16[256,2048]{1,0:T(8,128)(2,1)S(1)} %maximum_select_fusion.1), channel_id=1, source_target_pairs={{0,8},{1,9},{2,10},{3,11},{4,12},{5,13},{6,14},{7,15},{8,0},{9,1},... | collective-permute-start | bytes 3145736 | tf_op jit(solution)/shard_map/ppermute | solution.py:12
  31.4 19.2 %collective-permute-done.3 = bf16[256,2048]{1,0:T(8,128)(2,1)S(1)} collective-permute-done((bf16[256,2048]{1,0:T(8,128)(2,1)S(1)}, bf16[256,2048]{1,0:T(8,128)(2,1)S(1)}, u32[]{:S(2)}, u32[]{:S(2)}) %collective-permute-start.3) | collective-permute-done | bytes 1048608 | tf_op jit(solution)/shard_map/ppermute | solution.py:12
  51.4 2.3 %collective-permute-start.6 = (bf16[256,2]{0,1:T(2,128)(2,1)S(1)}, bf16[256,2]{0,1:T(2,128)(2,1)S(1)}, u32[]{:S(2)}, u32[]{:S(2)}) collective-permute-start(bf16[256,2]{0,1:T(2,128)(2,1)S(1)} %fusion.26), channel_id=1, source_target_pairs={{0,16},{1,17},{2,18},{3,19},{4,20},{5,21},{6,22},{7,23},{8,24},{9,... | collective-permute-start | bytes 3080 | tf_op jit(solution)/shard_map/ppermute | solution.py:12
  55.2 1.3 fusion.2
  56.5 2.3 %collective-permute-start.4 = (bf16[256,512]{1,0:T(8,128)(2,1)S(1)}, bf16[256,512]{1,0:T(8,128)(2,1)S(1)}, u32[]{:S(2)}, u32[]{:S(2)}) collective-permute-start(bf16[256,512]{1,0:T(8,128)(2,1)S(1)} %dynamic-slice_convert_fusion.3), channel_id=1, source_target_pairs={{0,16},{1,17},{2,18},{3,19},{4,20},{5,21},{6,22},{7,23},{8,24},{9,... | collective-permute-start | bytes 786440 | tf_op jit(solution)/shard_map/ppermute | solution.py:12
  58.9 1.9 %collective-permute-done.5 = bf16[256]{0:T(256)(128)(2,1)S(1)} collective-permute-done((bf16[256]{0:T(256)(128)(2,1)S(1)}, bf16[256]{0:T(256)(128)(2,1)S(1)}, u32[]{:S(2)}, u32[]{:S(2)}) %collective-permute-start.5) | collective-permute-done | bytes 544 | tf_op jit(solution)/shard_map/ppermute | solution.py:12
  60.9 7.8 %collective-permute-done.4 = bf16[256,512]{1,0:T(8,128)(2,1)S(1)} collective-permute-done((bf16[256,512]{1,0:T(8,128)(2,1)S(1)}, bf16[256,512]{1,0:T(8,128)(2,1)S(1)}, u32[]{:S(2)}, u32[]{:S(2)}) %collective-permute-start.4) | collective-permute-done | bytes 262176 | tf_op jit(solution)/shard_map/ppermute | solution.py:12
  69.7 1.3 copy.14
  71.0 1.3 copy.15
  73.4 20.3 %shard_map.131 = (f32[256,128,128]{2,1,0:T(8,128)}, f32[256,128]{1,0:T(8,128)}) custom-call(f32[256,128,128]{2,1,0:T(8,128)} %state_ref.1, f32[16,128,16]{2,1,0:T(8,128)} %bitcast.8, f32[16,128,16]{2,1,0:T(8,128)} %bitcast.9, f32[256,128]{1,0:T(8,128)} %get-tuple-element.11.value_ref, f32[3,256,128]{2,1,0:T(8,128)} %pad_maximum_fusion.rows_ref), custom_call_target="tpu_custom_call" | custom-call | tf_op jit(solution)/shard_map/pallas_call | solution.py:51
  93.8 1.0 multiply_convert_fusion.1
  94.9 2.9 %collective-permute-start.7 = (bf16[256,128]{1,0:T(8,128)(2,1)S(1)}, bf16[256,128]{1,0:T(8,128)(2,1)S(1)}, u32[]{:S(2)}, u32[]{:S(2)}) collective-permute-start(bf16[256,128]{1,0:T(8,128)(2,1)S(1)} %get-tuple-element.12), channel_id=1, source_target_pairs={{0,16},{1,17},{2,18},{3,19},{4,20},{5,21},{6,22},{7,23},{8,24},{9,... | collective-permute-start | bytes 196616 | tf_op jit(solution)/shard_map/ppermute | solution.py:12
  97.8 1.5 %collective-permute-done.8 = bf16[256]{0:T(256)(128)(2,1)S(1)} collective-permute-done((bf16[256]{0:T(256)(128)(2,1)S(1)}, bf16[256]{0:T(256)(128)(2,1)S(1)}, u32[]{:S(2)}, u32[]{:S(2)}) %collective-permute-start.8) | collective-permute-done | bytes 544 | tf_op jit(solution)/shard_map/ppermute | solution.py:12
  99.3 1.5 collective-permute-done.7
  101.6 2.0 %copy-done.1 = f32[512,2048]{1,0:T(8,128)} copy-done((f32[512,2048]{1,0:T(8,128)}, f32[512,2048]{1,0:T(8,128)S(1)}, u32[]{:S(2)}) %copy-start.1) | copy-done | bytes 4194328
  103.7 2.7 %collective-permute-start.9 = (bf16[256,2048]{1,0:T(8,128)(2,1)S(1)}, bf16[256,2048]{1,0:T(8,128)(2,1)}, u32[]{:S(2)}, u32[]{:S(2)}) collective-permute-start(bf16[256,2048]{1,0:T(8,128)(2,1)S(1)} %dynamic-slice_convert_fusion), channel_id=1, source_target_pairs={{0,8},{1,9},{2,10},{3,11},{4,12},{5,13},{6,14},{7,15},{8,0},{9,1},... | collective-permute-start | bytes 3145736 | tf_op jit(solution)/shard_map/ppermute | solution.py:12
  106.4 21.0 %collective-permute-done.9 = bf16[256,2048]{1,0:T(8,128)(2,1)} collective-permute-done((bf16[256,2048]{1,0:T(8,128)(2,1)S(1)}, bf16[256,2048]{1,0:T(8,128)(2,1)}, u32[]{:S(2)}, u32[]{:S(2)}) %collective-permute-start.9) | collective-permute-done | bytes 1048608 | tf_op jit(solution)/shard_map/ppermute | solution.py:12
  127.4 2.2 %convert_add_fusion = f32[256,2048]{1,0:T(8,128)S(1)} fusion(bf16[256,2048]{1,0:T(8,128)(2,1)} %collective-permute-done.9, f32[512,2048]{1,0:T(8,128)} %copy-done.1, s32[]{:T(128)S(6)} %select_n.184), kind=kLoop, calls=%fused_computation.14 | loop fusion | flops 1048576 | bytes 5242884 | tf_op jit(solution)/shard_map/add | solution.py:193
  129.6 1.5 collective-permute-start.10
  131.1 9.5 %collective-permute-done.10 = bf16[128,2048]{1,0:T(8,128)(2,1)} collective-permute-done((bf16[128,2048]{1,0:T(8,128)(2,1)S(1)}, bf16[128,2048]{1,0:T(8,128)(2,1)}, u32[]{:S(2)}, u32[]{:S(2)}) %collective-permute-start.10) | collective-permute-done | bytes 524320 | tf_op jit(solution)/shard_map/ppermute | solution.py:12
  140.6 1.1 convert_add_fusion.1
  141.8 1.0 copy-done.2
  142.8 1.3 collective-permute-start.11
  144.1 5.1 %collective-permute-done.11 = bf16[64,2048]{1,0:T(8,128)(2,1)S(1)} collective-permute-done((bf16[64,2048]{1,0:T(8,128)(2,1)S(1)}, bf16[64,2048]{1,0:T(8,128)(2,1)S(1)}, u32[]{:S(2)}, u32[]{:S(2)}) %collective-permute-start.11) | collective-permute-done | bytes 262176 | tf_op jit(solution)/shard_map/ppermute | solution.py:12
  149.2 1.1 convert_add_fusion.2
  150.4 1.3 collective-permute-done.12
  (58 shorter events, 9.5 us)
Async XLA Ops:
  0.6 100.2 %copy-start = (bf16[2048,128]{1,0:T(8,128)(2,1)S(1)}, bf16[2048,128]{1,0:T(8,128)(2,1)}, u32[]{:S(2)}) copy-start(bf16[2048,128]{1,0:T(8,128)(2,1)} %param.22) | copy-start | bytes 1572868
  0.6 29.5 %copy-start.9 = (f32[16]{0:T(128)S(1)}, f32[16]{0:T(128)}, u32[]{:S(2)}) copy-start(f32[16]{0:T(128)} %param.20) | copy-start | bytes 196
  0.7 30.7 %copy-start.10 = (bf16[128]{0:T(256)(128)(2,1)S(1)}, bf16[128]{0:T(256)(128)(2,1)}, u32[]{:S(2)}) copy-start(bf16[128]{0:T(256)(128)(2,1)} %param.21) | copy-start | bytes 772
  0.7 30.8 %copy-start.4 = (bf16[4096]{0:T(1024)(128)(2,1)S(1)}, bf16[4096]{0:T(1024)(128)(2,1)}, u32[]{:S(2)}) copy-start(bf16[4096]{0:T(1024)(128)(2,1)} %param.13) | copy-start | bytes 24580
  0.7 1.8 %collective-permute-start = (bf16[32,2048]{1,0:T(8,128)(2,1)}, bf16[32,2048]{1,0:T(8,128)(2,1)S(1)}, u32[]{:S(2)}, u32[]{:S(2)}) collective-permute-start(bf16[32,2048]{1,0:T(8,128)(2,1)} %param.12), channel_id=1, source_target_pairs={{0,1},{1,0},{2,3},{3,2},{4,5},{5,4},{6,7},{7,6},{8,9},{9,8},{10,11... | collective-permute-start | bytes 393224 | tf_op jit(solution)/shard_map/ppermute | solution.py:12
  3.5 9.5 %collective-permute-start.1 = (bf16[64,2048]{1,0:T(8,128)(2,1)S(1)}, bf16[64,2048]{1,0:T(8,128)(2,1)S(1)}, u32[]{:S(2)}, u32[]{:S(2)}) collective-permute-start(bf16[64,2048]{1,0:T(8,128)(2,1)S(1)} %maximum_select_fusion.3), channel_id=1, source_target_pairs={{0,2},{1,3},{2,0},{3,1},{4,6},{5,7},{6,4},{7,5},{8,10},{9,11},{10,... | collective-permute-start | bytes 786440 | tf_op jit(solution)/shard_map/ppermute | solution.py:12
  13.1 13.5 %collective-permute-start.2 = (bf16[128,2048]{1,0:T(8,128)(2,1)S(1)}, bf16[128,2048]{1,0:T(8,128)(2,1)S(1)}, u32[]{:S(2)}, u32[]{:S(2)}) collective-permute-start(bf16[128,2048]{1,0:T(8,128)(2,1)S(1)} %maximum_select_fusion.2), channel_id=1, source_target_pairs={{0,4},{1,5},{2,6},{3,7},{4,0},{5,1},{6,2},{7,3},{8,12},{9,13},{10,... | collective-permute-start | bytes 1572872 | tf_op jit(solution)/shard_map/ppermute | solution.py:12
  26.8 23.8 %collective-permute-start.3 = (bf16[256,2048]{1,0:T(8,128)(2,1)S(1)}, bf16[256,2048]{1,0:T(8,128)(2,1)S(1)}, u32[]{:S(2)}, u32[]{:S(2)}) collective-permute-start(bf16[256,2048]{1,0:T(8,128)(2,1)S(1)} %maximum_select_fusion.1), channel_id=1, source_target_pairs={{0,8},{1,9},{2,10},{3,11},{4,12},{5,13},{6,14},{7,15},{8,0},{9,1},... | collective-permute-start | bytes 3145736 | tf_op jit(solution)/shard_map/ppermute | solution.py:12
  51.3 3.9 %copy-start.5 = (bf16[2048,128]{1,0:T(8,128)(2,1)S(1)}, bf16[2048,128]{1,0:T(8,128)(2,1)}, u32[]{:S(2)}) copy-start(bf16[2048,128]{1,0:T(8,128)(2,1)} %param.17) | copy-start | bytes 1572868
  51.3 3.9 %copy-start.6 = (bf16[2048,128]{1,0:T(8,128)(2,1)S(1)}, bf16[2048,128]{1,0:T(8,128)(2,1)}, u32[]{:S(2)}) copy-start(bf16[2048,128]{1,0:T(8,128)(2,1)} %param.16) | copy-start | bytes 1572868
  51.3 3.9 %copy-start.7 = (bf16[2048,128]{1,0:T(8,128)(2,1)S(1)}, bf16[2048,128]{1,0:T(8,128)(2,1)}, u32[]{:S(2)}) copy-start(bf16[2048,128]{1,0:T(8,128)(2,1)} %param.15) | copy-start | bytes 1572868
  51.3 3.9 %copy-start.8 = (bf16[2048,128]{1,0:T(8,128)(2,1)S(1)}, bf16[2048,128]{1,0:T(8,128)(2,1)}, u32[]{:S(2)}) copy-start(bf16[2048,128]{1,0:T(8,128)(2,1)} %param.14) | copy-start | bytes 1572868
  51.4 9.5 %collective-permute-start.6 = (bf16[256,2]{0,1:T(2,128)(2,1)S(1)}, bf16[256,2]{0,1:T(2,128)(2,1)S(1)}, u32[]{:S(2)}, u32[]{:S(2)}) collective-permute-start(bf16[256,2]{0,1:T(2,128)(2,1)S(1)} %fusion.26), channel_id=1, source_target_pairs={{0,16},{1,17},{2,18},{3,19},{4,20},{5,21},{6,22},{7,23},{8,24},{9,... | collective-permute-start | bytes 3080 | tf_op jit(solution)/shard_map/ppermute | solution.py:12
  54.5 6.2 %collective-permute-start.5 = (bf16[256]{0:T(256)(128)(2,1)S(1)}, bf16[256]{0:T(256)(128)(2,1)S(1)}, u32[]{:S(2)}, u32[]{:S(2)}) collective-permute-start(bf16[256]{0:T(256)(128)(2,1)S(1)} %dynamic_slice.99), channel_id=1, source_target_pairs={{0,16},{1,17},{2,18},{3,19},{4,20},{5,21},{6,22},{7,23},{8,24},{9,... | collective-permute-start | bytes 1544 | tf_op jit(solution)/shard_map/ppermute | solution.py:12
  56.5 12.1 %collective-permute-start.4 = (bf16[256,512]{1,0:T(8,128)(2,1)S(1)}, bf16[256,512]{1,0:T(8,128)(2,1)S(1)}, u32[]{:S(2)}, u32[]{:S(2)}) collective-permute-start(bf16[256,512]{1,0:T(8,128)(2,1)S(1)} %dynamic-slice_convert_fusion.3), channel_id=1, source_target_pairs={{0,16},{1,17},{2,18},{3,19},{4,20},{5,21},{6,22},{7,23},{8,24},{9,... | collective-permute-start | bytes 786440 | tf_op jit(solution)/shard_map/ppermute | solution.py:12
  94.8 4.5 %collective-permute-start.8 = (bf16[256]{0:T(256)(128)(2,1)S(1)}, bf16[256]{0:T(256)(128)(2,1)S(1)}, u32[]{:S(2)}, u32[]{:S(2)}) collective-permute-start(bf16[256]{0:T(256)(128)(2,1)S(1)} %get-tuple-element.16), channel_id=1, source_target_pairs={{0,16},{1,17},{2,18},{3,19},{4,20},{5,21},{6,22},{7,23},{8,24},{9,... | collective-permute-start | bytes 1544 | tf_op jit(solution)/shard_map/ppermute | solution.py:12
  94.9 5.9 %collective-permute-start.7 = (bf16[256,128]{1,0:T(8,128)(2,1)S(1)}, bf16[256,128]{1,0:T(8,128)(2,1)S(1)}, u32[]{:S(2)}, u32[]{:S(2)}) collective-permute-start(bf16[256,128]{1,0:T(8,128)(2,1)S(1)} %get-tuple-element.12), channel_id=1, source_target_pairs={{0,16},{1,17},{2,18},{3,19},{4,20},{5,21},{6,22},{7,23},{8,24},{9,... | collective-permute-start | bytes 196616 | tf_op jit(solution)/shard_map/ppermute | solution.py:12
  101.5 2.0 %copy-start.1 = (f32[512,2048]{1,0:T(8,128)}, f32[512,2048]{1,0:T(8,128)S(1)}, u32[]{:S(2)}) copy-start(f32[512,2048]{1,0:T(8,128)S(1)} %convolution_multiply_fusion) | copy-start | bytes 12582916
  103.7 23.7 %collective-permute-start.9 = (bf16[256,2048]{1,0:T(8,128)(2,1)S(1)}, bf16[256,2048]{1,0:T(8,128)(2,1)}, u32[]{:S(2)}, u32[]{:S(2)}) collective-permute-start(bf16[256,2048]{1,0:T(8,128)(2,1)S(1)} %dynamic-slice_convert_fusion), channel_id=1, source_target_pairs={{0,8},{1,9},{2,10},{3,11},{4,12},{5,13},{6,14},{7,15},{8,0},{9,1},... | collective-permute-start | bytes 3145736 | tf_op jit(solution)/shard_map/ppermute | solution.py:12
  129.6 11.0 %collective-permute-start.10 = (bf16[128,2048]{1,0:T(8,128)(2,1)S(1)}, bf16[128,2048]{1,0:T(8,128)(2,1)}, u32[]{:S(2)}, u32[]{:S(2)}) collective-permute-start(bf16[128,2048]{1,0:T(8,128)(2,1)S(1)} %dynamic-slice_convert_fusion.1), channel_id=1, source_target_pairs={{0,4},{1,5},{2,6},{3,7},{4,0},{5,1},{6,2},{7,3},{8,12},{9,13},{10,... | collective-permute-start | bytes 1572872 | tf_op jit(solution)/shard_map/ppermute | solution.py:12
  131.1 20.7 %copy-start.3 = (bf16[32,2048]{1,0:T(8,128)(2,1)S(1)}, bf16[32,2048]{1,0:T(8,128)(2,1)}, u32[]{:S(2)}) copy-start(bf16[32,2048]{1,0:T(8,128)(2,1)} %param.12) | copy-start | bytes 393220
  141.8 1.0 copy-start.2
  142.8 6.4 %collective-permute-start.11 = (bf16[64,2048]{1,0:T(8,128)(2,1)S(1)}, bf16[64,2048]{1,0:T(8,128)(2,1)S(1)}, u32[]{:S(2)}, u32[]{:S(2)}) collective-permute-start(bf16[64,2048]{1,0:T(8,128)(2,1)S(1)} %dynamic-slice_convert_fusion.2), channel_id=1, source_target_pairs={{0,2},{1,3},{2,0},{3,1},{4,6},{5,7},{6,4},{7,5},{8,10},{9,11},{10,... | collective-permute-start | bytes 786440 | tf_op jit(solution)/shard_map/ppermute | solution.py:12
  150.4 1.4 collective-permute-start.12

commit v2 on v0

v2 whole, which is shorter than its diff:
```python
import functools

import jax
import jax.numpy as jnp
from jax import lax
from jax.experimental import pallas as pl
from jax.experimental.pallas import tpu as pltpu
from jax.sharding import PartitionSpec as P

EPS = 1e-06
MESH = pl.DeviceIdType.MESH
VMEM = pl.BlockSpec(memory_space=pltpu.VMEM)
SMALL = 16


def flip(me, bits):
    other = me
    for bit in bits:
        other = other + (1 - 2 * ((me // (1 << bit)) % 2)) * (1 << bit)
    return other


def parts_of(cols, dims):
    tiles = cols // 128
    count = max(1, min(dims, tiles))
    cuts = [tiles * i // count * 128 for i in range(count + 1)]
    ranges = [(cuts[i], cuts[i + 1] - cuts[i]) for i in range(count)]
    orders = [[1 + (i + j) % dims for j in range(dims)] for i in range(count)]
    return list(zip(ranges, orders))


def masks_of(order):
    sets = [((), -1)]
    for step in range(len(order)):
        sets = sets + [(bits + (order[step],), step) for bits, _ in sets]
    return sets


def key_of(bits):
    return sum(1 << (bit - 1) for bit in bits)


def enter(devices):
    barrier = pltpu.get_barrier_semaphore()
    for device in devices:
        pl.semaphore_signal(barrier, inc=1, device_id=(device,), device_id_type=MESH)
    pl.semaphore_wait(barrier, len(devices))


def remote(source, target, send_sem, recv_sem, device):
    return pltpu.make_async_remote_copy(
        src_ref=source,
        dst_ref=target,
        send_sem=send_sem,
        recv_sem=recv_sem,
        device_id=(device,),
        device_id_type=MESH,
    )


def project_kernel(
    heads,
    groups,
    stream_ref,
    gain_ref,
    query_w,
    key_w,
    value_w,
    gate_w,
    write_w,
    decay_w,
    rate_ref,
    query_out,
    key_out,
    value_out,
    gate_out,
    side_out,
    gathered,
    partial,
    sent,
    received,
    small_sent,
    small_received,
    turned,
    ici_send,
    ici_recv,
    core_send,
    core_recv,
    group_send,
    group_recv,
    small_send,
    small_recv,
):
    me = lax.axis_index("tp")
    place = me % heads
    group = me // heads
    rows, cols = stream_ref.shape
    batch = gathered.shape[0]
    group_rows = batch // groups
    dims = heads.bit_length() - 2
    sibling = flip(me, (0,))
    neighbours = [flip(me, (bit,)) for bit in range(1, dims + 1)]
    others = [place + heads * ((group + j) % groups) for j in range(1, groups)]
    enter([sibling] + neighbours + others)

    def block(device_place, part):
        (start, width), _ = part
        begin = pl.multiple_of(device_place * rows, rows)
        return gathered.at[pl.ds(begin, rows), pl.ds(start, width)]

    parts = parts_of(cols, dims)
    sends = []
    arrivals = []
    core_copies = []

    def pass_on(p, part, bits, step):
        order = part[1]
        origin = flip(place, bits)
        if bits:
            source = block(origin, part)
        else:
            source = stream_ref.at[:, pl.ds(part[0][0], part[0][1])]
        for later in range(step + 1, dims):
            landed = key_of(bits + (order[later],))
            copy = remote(
                source,
                block(origin, part),
                ici_send.at[p, landed],
                ici_recv.at[p, landed],
                flip(me, (order[later],)),
            )
            copy.start()
            sends.append(copy)
        own = key_of(bits)
        copy = remote(
            source, block(origin, part), core_send.at[p, own], core_recv.at[p, own], sibling
        )
        copy.start()
        core_copies.append(copy)

    def arrived(p, part, bits):
        landed = key_of(bits)
        target = block(flip(place, bits), part)
        remote(target, target, ici_send.at[p, landed], ici_recv.at[p, landed], sibling).wait_recv()

    for p, part in enumerate(parts):
        pass_on(p, part, (), -1)
    own_rows = pl.ds(pl.multiple_of(place * rows, rows), rows)
    gathered[own_rows, :] = stream_ref[...]
    for index in range(1, 1 << dims):
        for p, part in enumerate(parts):
            bits, step = masks_of(part[1])[index]
            arrived(p, part, bits)
            pass_on(p, part, bits, step)
    for copy in core_copies:
        copy.wait_recv()

    gain = gain_ref[group].astype(jnp.float32)
    write_block = write_w[group]
    decay_block = decay_w[group]
    size = query_w.shape[1]

    def project(begin, count, at):
        x = gathered[pl.ds(begin, count), :].astype(jnp.float32)
        gained = (x * gain).astype(jnp.bfloat16)
        for i, weight in enumerate((query_w, key_w, value_w, gate_w)):
            partial[pl.ds(at, count), i * size : (i + 1) * size] = jnp.dot(
                gained, weight[...], preferred_element_type=jnp.float32
            )
        mine = lax.broadcasted_iota(jnp.int32, (count, heads), 1) == place
        pre = [
            jnp.sum(
                jnp.where(mine, jnp.dot(gained, w, preferred_element_type=jnp.float32), 0.0),
                axis=1,
                keepdims=True,
            )
            for w in (write_block, decay_block)
        ]
        squares = jnp.sum(x * x, axis=1, keepdims=True)
        lane = lax.broadcasted_iota(jnp.int32, (count, 128), 1)
        return jnp.where(
            lane == 0, pre[0], jnp.where(lane == 1, pre[1], jnp.where(lane == 2, squares, 0.0))
        )

    copies = []
    wide = max(group_rows, 128)
    for j in list(range(1, groups)) + [0]:
        target_group = (group + j) % groups
        begin = pl.multiple_of(target_group * group_rows, group_rows)
        side = project(begin, group_rows, 0)
        if j:
            sent[j - 1] = partial[...].astype(jnp.bfloat16)
            turned[0:group_rows, :] = side
            flat = turned[...].T
            small_sent[j - 1] = flat[0:SMALL, 0:group_rows].astype(jnp.bfloat16)
            for source, target, send, recv in (
                (sent, received, group_send, group_recv),
                (small_sent, small_received, small_send, small_recv),
            ):
                copy = remote(
                    source.at[j - 1],
                    target.at[j - 1],
                    send.at[j - 1],
                    recv.at[j - 1],
                    others[j - 1],
                )
                copy.start()
                copies.append(copy)
    total = partial[...]
    turned[0:group_rows, :] = side
    flat = turned[...].T[0:SMALL, :]
    for copy in copies:
        copy.wait_recv()
    for j in range(1, groups):
        total = total + received[j - 1].astype(jnp.float32)
    small_total = flat[:, 0:group_rows]
    for j in range(1, groups):
        small_total = small_total + small_received[j - 1].astype(jnp.float32)
    turned_back = jnp.concatenate(
        [small_total, jnp.zeros((SMALL, wide - group_rows), jnp.float32)], axis=1
    ) if wide > group_rows else small_total
    side = jnp.concatenate(
        [turned_back, jnp.zeros((128 - SMALL, wide), jnp.float32)], axis=0
    ).T[0:group_rows]
    scale = lax.rsqrt(side[:, 2:3] / (cols * groups) + EPS)

    def rounded(v):
        return v.astype(jnp.bfloat16).astype(jnp.float32)

    projected = rounded(total * scale)
    query = projected[:, :size]
    key = projected[:, size : 2 * size]
    query = query * lax.rsqrt(jnp.sum(query * query, axis=1, keepdims=True) + EPS) * size**-0.5
    key = key * lax.rsqrt(jnp.sum(key * key, axis=1, keepdims=True) + EPS)
    query_out[...] = query
    key_out[...] = key
    value_out[...] = projected[:, 2 * size : 3 * size]
    gate_out[...] = projected[:, 3 * size :]
    pre = rounded(side * scale)
    strength = jax.nn.sigmoid(pre[:, 0:1])
    mine = lax.broadcasted_iota(jnp.int32, rate_ref.shape, 1) == place
    rate = jnp.sum(jnp.where(mine, rate_ref[...], 0.0), axis=1, keepdims=True)
    decay = pre[:, 1:2]
    softplus = jnp.maximum(decay, 0.0) + jnp.log(1.0 + jnp.exp(-jnp.abs(decay)))
    factor = jnp.exp(-rate * softplus)
    overlap = jnp.sum(query * key, axis=1, keepdims=True)
    side_out[0] = jnp.broadcast_to(strength, (group_rows, size))
    side_out[1] = jnp.broadcast_to(factor, (group_rows, size))
    side_out[2] = jnp.broadcast_to(overlap, (group_rows, size))
    for copy in sends + core_copies + copies:
        copy.wait_send()


def project(stream, norm_gain, weights, write_weight, decay_weight, rate, heads, groups):
    rows, cols = stream.shape
    batch = rows * heads
    group_rows = batch // groups
    size = weights[0].shape[1]
    dims = heads.bit_length() - 2
    parts = len(parts_of(cols, dims))
    extra = groups - 1
    dma = pltpu.SemaphoreType.DMA
    vec = jax.ShapeDtypeStruct((group_rows, size), jnp.float32)
    return pl.pallas_call(
        functools.partial(project_kernel, heads, groups),
        in_specs=[VMEM] * 9,
        out_specs=[VMEM] * 5,
        out_shape=[vec] * 4 + [jax.ShapeDtypeStruct((3, group_rows, size), jnp.float32)],
        scratch_shapes=[
            pltpu.VMEM((batch, cols), jnp.bfloat16),
            pltpu.VMEM((group_rows, 4 * size), jnp.float32),
            pltpu.VMEM((extra, group_rows, 4 * size), jnp.bfloat16),
            pltpu.VMEM((extra, group_rows, 4 * size), jnp.bfloat16),
            pltpu.VMEM((extra, SMALL, group_rows), jnp.bfloat16),
            pltpu.VMEM((extra, SMALL, group_rows), jnp.bfloat16),
            pltpu.VMEM((max(group_rows, 128), 128), jnp.float32),
            dma((parts, 1 << dims)),
            dma((parts, 1 << dims)),
            dma((parts, 1 << dims)),
            dma((parts, 1 << dims)),
            dma((extra,)),
            dma((extra,)),
            dma((extra,)),
            dma((extra,)),
        ],
        compiler_params=pltpu.CompilerParams(
            collective_id=0, has_side_effects=True, vmem_limit_bytes=48 * 1024 * 1024
        ),
    )(
        stream,
        norm_gain.reshape(groups, 1, cols),
        *weights,
        write_weight.reshape(groups, cols, heads),
        decay_weight.reshape(groups, cols, heads),
        rate.reshape(1, heads),
    )


def split(v):
    high = v.astype(jnp.bfloat16)
    return high, (v - high.astype(jnp.float32)).astype(jnp.bfloat16)


def state_kernel(state_ref, key_ref, query_ref, value_ref, side_ref, new_ref, read_ref):
    count, size, _ = state_ref.shape
    key_high, key_low = split(key_ref[...])
    query_high, query_low = split(query_ref[...])
    spots = lax.broadcasted_iota(jnp.int32, (count, size), 0)
    recalled = jnp.zeros((count, size), jnp.float32)
    asked = jnp.zeros((count, size), jnp.float32)
    four = jnp.concatenate([key_high, key_low, query_high, query_low], axis=0)
    for b in range(count):
        memory = state_ref[b].astype(jnp.bfloat16)
        both = jnp.dot(four, memory, preferred_element_type=jnp.float32)
        recalled = jnp.where(spots == b, both[0:count] + both[count : 2 * count], recalled)
        asked = jnp.where(
            spots == b, both[2 * count : 3 * count] + both[3 * count : 4 * count], asked
        )
    strength, factor, overlap = side_ref[0], side_ref[1], side_ref[2]
    change = strength * (value_ref[...] - factor * recalled)
    read_ref[...] = factor * asked + overlap * change
    change_high, change_low = split(change)
    left = jnp.concatenate([key_high, key_low, key_high], axis=0)
    right = jnp.concatenate([change_high, change_high, change_low], axis=0)
    wide_spots = lax.broadcasted_iota(jnp.int32, right.shape, 0) % count
    for b in range(count):
        only = jnp.where(wide_spots == b, right.astype(jnp.float32), 0.0).astype(jnp.bfloat16)
        outer = lax.dot_general(
            left, only, (((0,), (0,)), ((), ())), preferred_element_type=jnp.float32
        )
        new_ref[b] = factor[b : b + 1, :] * state_ref[b] + outer


def state_step(state, query, key, value, side):
    count, size, _ = state.shape
    block = min(16, count)
    row_spec = pl.BlockSpec((block, size), lambda i: (i, 0))
    return pl.pallas_call(
        state_kernel,
        grid=(count // block,),
        in_specs=[
            pl.BlockSpec((block, size, size), lambda i: (i, 0, 0)),
            row_spec,
            row_spec,
            row_spec,
            pl.BlockSpec((3, block, size), lambda i: (0, i, 0)),
        ],
        out_specs=[pl.BlockSpec((block, size, size), lambda i: (i, 0, 0)), row_spec],
        out_shape=[
            jax.ShapeDtypeStruct(state.shape, state.dtype),
            jax.ShapeDtypeStruct((count, size), jnp.float32),
        ],
    )(state, key, query, value, side)


def output_kernel(
    heads,
    groups,
    stream_ref,
    gated_ref,
    scaling_ref,
    weight_ref,
    out_ref,
    all_gated,
    all_scaling,
    columns,
    held,
    core_out,
    core_in,
    hop_out,
    hop_in,
    gated_send,
    gated_recv,
    scaling_send,
    scaling_recv,
    core_send,
    core_recv,
    hop_send,
    hop_recv,
):
    me = lax.axis_index("tp")
    place = me % heads
    group = me // heads
    rows, cols = stream_ref.shape
    batch = all_gated.shape[0]
    group_rows = batch // groups
    dims = heads.bit_length() - 2
    chips = 1 << dims
    sibling = flip(me, (0,))
    neighbours = [flip(me, (bit,)) for bit in range(1, dims + 1)]
    others = [place + heads * ((group + j) % groups) for j in range(1, groups)]
    enter([sibling] + neighbours + others)
    own_rows = pl.ds(pl.multiple_of(group * group_rows, group_rows), group_rows)
    copies = []
    arriving = []
    for j in range(1, groups):
        for source, target, send, recv in (
            (gated_ref, all_gated.at[own_rows], gated_send, gated_recv),
            (scaling_ref, all_scaling.at[group], scaling_send, scaling_recv),
        ):
            copy = remote(source, target, send.at[j - 1], recv.at[j - 1], others[j - 1])
            copy.start()
            copies.append(copy)
    all_gated[own_rows, :] = gated_ref[...]
    all_scaling[group] = scaling_ref[...]
    for copy in copies:
        copy.wait_recv()
    wide = max(group_rows, 128)
    for g in range(groups):
        flat = all_scaling[g].astype(jnp.float32)
        if wide > group_rows:
            flat = jnp.concatenate(
                [flat, jnp.zeros((SMALL, wide - group_rows), jnp.float32)], axis=1
            )
        flat = jnp.concatenate([flat, jnp.zeros((128 - SMALL, wide), jnp.float32)], axis=0)
        columns[g * group_rows : (g + 1) * group_rows, :] = flat.T[0:group_rows]

    def relative(owner, mask):
        bits = tuple(bit for bit in range(1, dims + 1) if mask >> (bit - 1) & 1)
        begin = flip(owner, bits) * rows
        return pl.ds(pl.multiple_of(begin, rows), rows)

    def head_rows(owner, masks):
        picks = [relative(owner, mask) for mask in masks]
        left = jnp.concatenate([all_gated[pick, :] for pick in picks], axis=0)
        scale = jnp.concatenate([columns[pick, 0:1] for pick in picks], axis=0)
        product = lax.dot_general(
            left, weight_ref[...], (((1,), (1,)), ((), ())), preferred_element_type=jnp.float32
        )
        return product * scale

    core_copies = [
        remote(
            core_out.at[mask], core_in.at[mask], core_send.at[mask], core_recv.at[mask], sibling
        )
        for mask in range(chips)
    ]
    batch_of = min(4, chips)
    sweep = list(range(chips - 1, -1, -1))
    for first in range(0, chips, batch_of):
        masks = sweep[first : first + batch_of]
        product = head_rows(flip(place, (0,)), masks).astype(jnp.bfloat16)
        for i, mask in enumerate(masks):
            core_out[mask] = product[i * rows : (i + 1) * rows]
            core_copies[mask].start()
    for first in range(0, chips, batch_of):
        masks = sweep[first : first + batch_of]
        product = head_rows(place, masks)
        for i, mask in enumerate(masks):
            held[mask] = product[i * rows : (i + 1) * rows]
    for mask in sweep:
        core_copies[mask].wait_recv()
        held[mask] += core_in[mask].astype(jnp.float32)

    parts = parts_of(cols, dims)
    hops = []
    for step in range(dims):
        started = []
        for p, ((start, width), order) in enumerate(parts):
            span = pl.ds(start, width)
            crossed = [1 << (bit - 1) for bit in order[:step]]
            now = 1 << (order[step] - 1)
            for mask in range(chips):
                if any(mask & c for c in crossed) or not mask & now:
                    continue
                landed = mask - now
                hop_out[step, landed, :, span] = held[mask, :, span].astype(jnp.bfloat16)
                copy = remote(
                    hop_out.at[step, landed, :, span],
                    hop_in.at[step, landed, :, span],
                    hop_send.at[step, p, landed],
                    hop_recv.at[step, p, landed],
                    neighbours[order[step] - 1],
                )
                copy.start()
                started.append((landed, span, copy))
        for landed, span, copy in started:
            copy.wait_recv()
            held[landed, :, span] += hop_in[step, landed, :, span].astype(jnp.float32)
            hops.append(copy)
    out_ref[...] = (stream_ref[...].astype(jnp.float32) + held[0]).astype(jnp.bfloat16)
    for copy in copies + core_copies + hops:
        copy.wait_send()


def output(stream, gated, scaling, out_weight, heads, groups):
    rows, cols = stream.shape
    batch = rows * heads
    group_rows, size = gated.shape
    dims = heads.bit_length() - 2
    chips = 1 << dims
    parts = len(parts_of(cols, dims))
    extra = groups - 1
    dma = pltpu.SemaphoreType.DMA
    flat = jnp.broadcast_to(scaling.astype(jnp.bfloat16)[None, :], (SMALL, group_rows))
    return pl.pallas_call(
        functools.partial(output_kernel, heads, groups),
        in_specs=[VMEM] * 4,
        out_specs=VMEM,
        out_shape=jax.ShapeDtypeStruct(stream.shape, stream.dtype),
        scratch_shapes=[
            pltpu.VMEM((batch, size), jnp.bfloat16),
            pltpu.VMEM((groups, SMALL, group_rows), jnp.bfloat16),
            pltpu.VMEM((batch, 128), jnp.float32),
            pltpu.VMEM((chips, rows, cols), jnp.float32),
            pltpu.VMEM((chips, rows, cols), jnp.bfloat16),
            pltpu.VMEM((chips, rows, cols), jnp.bfloat16),
            pltpu.VMEM((dims, chips, rows, cols), jnp.bfloat16),
            pltpu.VMEM((dims, chips, rows, cols), jnp.bfloat16),
            dma((extra,)),
            dma((extra,)),
            dma((extra,)),
            dma((extra,)),
            dma((chips,)),
            dma((chips,)),
            dma((dims, parts, chips)),
            dma((dims, parts, chips)),
        ],
        compiler_params=pltpu.CompilerParams(
            collective_id=1, has_side_effects=True, vmem_limit_bytes=48 * 1024 * 1024
        ),
    )(stream, gated, flat, out_weight)


def per_device(
    stream,
    norm_gain,
    query_weight,
    key_weight,
    value_weight,
    gate_weight,
    write_weight,
    decay_weight,
    decay_rate,
    head_gain,
    out_weight,
    state,
):
    heads = decay_rate.shape[0]
    groups = lax.axis_size("tp") // heads
    weights = (query_weight, key_weight, value_weight, gate_weight)
    query, key, value, gate, side = project(
        stream, norm_gain, weights, write_weight, decay_weight, decay_rate, heads, groups
    )
    updated, readout = state_step(state, query, key, value, side)
    scaling = lax.rsqrt(jnp.mean(readout * readout, axis=1) + EPS)
    gated = (readout * head_gain.astype(jnp.float32)[None, :] * jax.nn.silu(gate)).astype(
        jnp.bfloat16
    )
    result = output(stream, gated, scaling, out_weight, heads, groups)
    return (result, updated)


def solution(mesh):
    placed = (
        P("tp", None),
        P(),
        P("tp", None),
        P("tp", None),
        P("tp", None),
        P("tp", None),
        P(),
        P(),
        P(),
        P(),
        P("tp", None),
        P("tp", None, None),
    )
    return jax.shard_map(
        per_device,
        mesh=mesh,
        in_specs=placed,
        out_specs=(P("tp", None), P("tp", None, None)),
        check_vma=False,
    )
```

time: 163 us -> 94.6 us (0.58)
  waiting for transfers between devices: 86.2 us -> 0 us
  Pallas kernels: 0 us -> 79.4 us
  matrix products: 31.9 us -> 0 us
  starting transfers between devices: 20.9 us -> 0 us
  other arithmetic: 15.5 us -> 1.03 us
  local copies, waits for them, and re-layouts: 6.29 us -> 12.6 us
    ppermute x13 -> x0, waiting for transfers between devices: 86.2 us -> none  [from_partner(): lax.ppermute(shard, axis, [(i, i ^ 1 << bit) for i in range(lax.axis_size...]
    pallas_call x0 -> x3, Pallas kernels: none -> 79.4 us  [the longest x1 33.7 us: project(): pl.pallas_call(functools.partial(project_kernel, heads, groups), in_specs...]
    dot_general x5 -> x0, matrix products: 31.9 us -> none  [the longest x1 14.7 us: per_device(): recalled = jnp.einsum('bdj,bd->bj', state, key_vec, precision=highest)]
    ppermute x13 -> x0, starting transfers between devices: 20.9 us -> none  [from_partner(): lax.ppermute(shard, axis, [(i, i ^ 1 << bit) for i in range(lax.axis_size...]
    add x4 -> x0, other arithmetic: 10.5 us -> none  [the longest x1 6.11 us: per_device(): decay_factor[:, None, None] * state]
    unnamed x26 -> x29, local copies, waits for them, and re-layouts: 2.98 us -> 11.9 us
    dynamic_slice x4 -> x0, local copies, waits for them, and re-layouts: 3.01 us -> none  [the longest x1 1.24 us: per_device(): rate_value = lax.dynamic_slice_in_dim(decay_rate, my_head, 1, 0)[0]]
  transfers between devices with their start and end apart: 13 -> 0, of which waited for: 12 -> 0; matrix products, arithmetic and copies ran while one was open for 4% -> 0% of each run, Pallas kernels for 0% -> 0%
where the time goes in v2:
time: 94.6 us; the launch traced here: 93.8 us
  Pallas kernels  79.4 us (84%)
  local copies, waits for them, and re-layouts  12.6 us (13%)
  other arithmetic  1.03 us (1%)
    pallas_call x1, Pallas kernels, project(): pl.pallas_call(functools.partial(project_kernel, heads, groups), in_specs...  33.7 us
    pallas_call x1, Pallas kernels, output(): pl.pallas_call(functools.partial(output_kernel, heads, groups), in_specs=...  24.7 us
    pallas_call x1, Pallas kernels, state_step(): pl.pallas_call(state_kernel, grid=(count // block,), in_specs=[pl.BlockSp...  21.1 us
    unnamed x29, local copies, waits for them, and re-layouts  11.9 us

profile of v2, /device:TPU:0, one launch (start us, length us, event | category | flops | bytes accessed | tf_op | source)
XLA Modules:
  0.0 93.8 jit_solution(6214612775894124688)
XLA Ops:
  0.6 0.0 copy-start.6
  0.6 0.0 copy-start.12
  0.7 0.0 copy-start.4
  0.7 1.4 %copy.16 = bf16[4096,16]{1,0:T(8,128)(2,1)S(1)} copy(bf16[4096,16]{0,1:T(8,128)(2,1)} %param.18) | data formatting | bytes 262144 | tf_op args[6]
  2.1 1.4 %copy.17 = bf16[4096,16]{1,0:T(8,128)(2,1)S(1)} copy(bf16[4096,16]{0,1:T(8,128)(2,1)} %param.19) | data formatting | bytes 262144 | tf_op args[7]
  3.5 0.7 reshape.27.gain_ref
  4.2 0.0 copy-start
  4.2 1.0 %copy-done = bf16[2048,128]{1,0:T(8,128)(2,1)S(1)} copy-done((bf16[2048,128]{1,0:T(8,128)(2,1)S(1)}, bf16[2048,128]{1,0:T(8,128)(2,1)}, u32[]{:S(2)}) %copy-start) | copy-done | bytes 524312
  5.3 0.0 copy-start.1
  5.3 1.0 %copy-done.1 = bf16[2048,128]{1,0:T(8,128)(2,1)S(1)} copy-done((bf16[2048,128]{1,0:T(8,128)(2,1)S(1)}, bf16[2048,128]{1,0:T(8,128)(2,1)}, u32[]{:S(2)}) %copy-start.1) | copy-done | bytes 524312
  6.3 0.0 copy-start.2
  6.3 1.0 %copy-done.2 = bf16[2048,128]{1,0:T(8,128)(2,1)S(1)} copy-done((bf16[2048,128]{1,0:T(8,128)(2,1)S(1)}, bf16[2048,128]{1,0:T(8,128)(2,1)}, u32[]{:S(2)}) %copy-start.2) | copy-done | bytes 524312
  7.3 0.0 copy-start.3
  7.3 1.0 %copy-done.3 = bf16[2048,128]{1,0:T(8,128)(2,1)S(1)} copy-done((bf16[2048,128]{1,0:T(8,128)(2,1)S(1)}, bf16[2048,128]{1,0:T(8,128)(2,1)}, u32[]{:S(2)}) %copy-start.3) | copy-done | bytes 524312
  8.4 0.0 copy-start.5
  8.4 0.9 copy-done.5
  9.3 0.0 copy-start.11
  9.3 0.7 copy-done.11
  9.9 33.7 %shard_map.131 = (f32[256,128]{1,0:T(8,128)S(1)}, f32[256,128]{1,0:T(8,128)S(1)}, f32[256,128]{1,0:T(8,128)S(1)}, f32[256,128]{1,0:T(8,128)S(1)}, f32[3,256,128]{2,1,0:T(8,128)S(1)}) custom-call(bf16[32,2048]{1,0:T(8,128)(2,1)S(1)} %copy-done.5, bf16[2,1,2048]{2,1,0:T(2,128)(2,1)S(1)} %reshape.27.gain_ref, bf16[2048,128]{1,0:T(8,128)(2,1)S(1)} %copy-done, ...), custom_call_target="tpu_custom_call" | custom-call | tf_op jit(solution)/shard_map/pallas_call | solution.py:264
  43.7 0.0 copy-start.7
  43.7 0.7 copy-done.7
  44.4 0.0 copy-start.8
  44.4 0.6 copy-done.8
  45.1 0.7 copy-done.9
  45.7 0.6 copy-done.10
  46.3 21.1 %shard_map.132 = (f32[256,128,128]{2,1,0:T(8,128)}, f32[256,128]{1,0:T(8,128)}) custom-call(f32[256,128,128]{2,1,0:T(8,128)} %state_ref.1, f32[256,128]{1,0:T(8,128)} %copy-done.9, f32[256,128]{1,0:T(8,128)} %copy-done.8, f32[256,128]{1,0:T(8,128)} %copy-done.10, f32[3,256,128]{2,1,0:T(8,128)} %copy-done.7), custom_call_target="tpu_custom_call" | custom-call | tf_op jit(solution)/shard_map/pallas_call | solution.py:338
  67.4 0.0 copy-done.12
  67.4 1.0 %multiply_reduce_fusion = (f32[256]{0:T(256)S(1)}, bf16[256,128]{1,0:T(8,128)(2,1)S(1)}) fusion(f32[256,128]{1,0:T(8,128)} %get-tuple-element.13, f32[256,128]{1,0:T(8,128)S(1)} %get-tuple-element.14, f32[128]{0:T(128)S(1)} %convert_element_type.13), kind=kLoop, calls=%fused_computation | loop fusion | flops 294656 | bytes 329216 | tf_op jit(solution)/shard_map/reduce_sum | solution.py:546
  68.5 0.0 copy-done.6
  68.5 0.0 copy-done.4
  68.5 24.7 %shard_map.133 = bf16[32,2048]{1,0:T(8,128)(2,1)S(1)} custom-call(bf16[32,2048]{1,0:T(8,128)(2,1)S(1)} %copy-done.6, bf16[256,128]{1,0:T(8,128)(2,1)S(1)} %get-tuple-element.17.gated_ref, bf16[16,256]{1,0:T(8,128)(2,1)S(1)} %broadcast_in_dim.2.scaling_ref, bf16[2048,128]{1,0:T(8,128)(2,1)S(1)} %copy-done.4), custom_call_target="tpu_custom_call" | custom-call | tf_op jit(solution)/shard_map/pallas_call | solution.py:496
  93.2 0.7 copy.20
  (5 shorter events, 0.0 us)
Async XLA Ops:
  0.6 67.8 %copy-start.6 = (bf16[32,2048]{1,0:T(8,128)(2,1)S(1)}, bf16[32,2048]{1,0:T(8,128)(2,1)}, u32[]{:S(2)}) copy-start(bf16[32,2048]{1,0:T(8,128)(2,1)} %stream_ref.3) | copy-start | bytes 393220
  0.6 66.8 %copy-start.12 = (bf16[128]{0:T(256)(128)(2,1)S(1)}, bf16[128]{0:T(256)(128)(2,1)}, u32[]{:S(2)}) copy-start(bf16[128]{0:T(256)(128)(2,1)} %param.21) | copy-start | bytes 772
  0.7 67.8 %copy-start.4 = (bf16[2048,128]{1,0:T(8,128)(2,1)S(1)}, bf16[2048,128]{1,0:T(8,128)(2,1)}, u32[]{:S(2)}) copy-start(bf16[2048,128]{1,0:T(8,128)(2,1)} %weight_ref.1) | copy-start | bytes 1572868
  4.2 1.0 %copy-start = (bf16[2048,128]{1,0:T(8,128)(2,1)S(1)}, bf16[2048,128]{1,0:T(8,128)(2,1)}, u32[]{:S(2)}) copy-start(bf16[2048,128]{1,0:T(8,128)(2,1)} %query_w.1) | copy-start | bytes 1572868
  5.3 1.0 %copy-start.1 = (bf16[2048,128]{1,0:T(8,128)(2,1)S(1)}, bf16[2048,128]{1,0:T(8,128)(2,1)}, u32[]{:S(2)}) copy-start(bf16[2048,128]{1,0:T(8,128)(2,1)} %key_w.1) | copy-start | bytes 1572868
  6.3 1.0 %copy-start.2 = (bf16[2048,128]{1,0:T(8,128)(2,1)S(1)}, bf16[2048,128]{1,0:T(8,128)(2,1)}, u32[]{:S(2)}) copy-start(bf16[2048,128]{1,0:T(8,128)(2,1)} %value_w.1) | copy-start | bytes 1572868
  7.3 1.0 %copy-start.3 = (bf16[2048,128]{1,0:T(8,128)(2,1)S(1)}, bf16[2048,128]{1,0:T(8,128)(2,1)}, u32[]{:S(2)}) copy-start(bf16[2048,128]{1,0:T(8,128)(2,1)} %gate_w.1) | copy-start | bytes 1572868
  8.4 0.9 copy-start.5
  9.3 0.7 copy-start.11
  43.7 0.7 copy-start.7
  44.4 0.6 copy-start.8
  45.0 0.7 copy-start.9
  45.7 0.6 copy-start.10

commit v3 on v2

--- a/solution.py
+++ b/solution.py
@@ -70,12 +70,12 @@
     write_w,
     decay_w,
     rate_ref,
-    query_out,
-    key_out,
-    value_out,
-    gate_out,
-    side_out,
+    packed_out,
     gathered,
+    weights,
+    write_t,
+    decay_t,
+    local_sems,
     partial,
     sent,
     received,
@@ -101,6 +101,19 @@
     sibling = flip(me, (0,))
     neighbours = [flip(me, (bit,)) for bit in range(1, dims + 1)]
     others = [place + heads * ((group + j) % groups) for j in range(1, groups)]
+    size = query_w.shape[1]
+    own_cols = pl.ds(pl.multiple_of(group * cols, cols), cols)
+    fetches = [
+        pltpu.make_async_copy(
+            weight, weights.at[:, i * size : (i + 1) * size], local_sems.at[i]
+        )
+        for i, weight in enumerate((query_w, key_w, value_w, gate_w))
+    ] + [
+        pltpu.make_async_copy(source.at[:, own_cols], target, local_sems.at[4 + i])
+        for i, (source, target) in enumerate(((write_w, write_t), (decay_w, decay_t)))
+    ]
+    for fetch in fetches:
+        fetch.start()
     enter([sibling] + neighbours + others)
 
     def block(device_place, part):
@@ -156,25 +169,32 @@
         copy.wait_recv()
 
     gain = gain_ref[group].astype(jnp.float32)
-    write_block = write_w[group]
-    decay_block = decay_w[group]
-    size = query_w.shape[1]
+    for fetch in fetches:
+        fetch.wait()
 
     def project(begin, count, at):
         x = gathered[pl.ds(begin, count), :].astype(jnp.float32)
         gained = (x * gain).astype(jnp.bfloat16)
-        for i, weight in enumerate((query_w, key_w, value_w, gate_w)):
-            partial[pl.ds(at, count), i * size : (i + 1) * size] = jnp.dot(
-                gained, weight[...], preferred_element_type=jnp.float32
-            )
+        partial[pl.ds(at, count), :] = jnp.dot(
+            gained, weights[...], preferred_element_type=jnp.float32
+        )
         mine = lax.broadcasted_iota(jnp.int32, (count, heads), 1) == place
         pre = [
             jnp.sum(
-                jnp.where(mine, jnp.dot(gained, w, preferred_element_type=jnp.float32), 0.0),
+                jnp.where(
+                    mine,
+                    lax.dot_general(
+                        gained,
+                        w[...],
+                        (((1,), (1,)), ((), ())),
+                        preferred_element_type=jnp.float32,
+                    ),
+                    0.0,
+                ),
                 axis=1,
                 keepdims=True,
             )
-            for w in (write_block, decay_block)
+            for w in (write_t, decay_t)
         ]
         squares = jnp.sum(x * x, axis=1, keepdims=True)
         lane = lax.broadcasted_iota(jnp.int32, (count, 128), 1)
@@ -232,10 +252,9 @@
     key = projected[:, size : 2 * size]
     query = query * lax.rsqrt(jnp.sum(query * query, axis=1, keepdims=True) + EPS) * size**-0.5
     key = key * lax.rsqrt(jnp.sum(key * key, axis=1, keepdims=True) + EPS)
-    query_out[...] = query
-    key_out[...] = key
-    value_out[...] = projected[:, 2 * size : 3 * size]
-    gate_out[...] = projected[:, 3 * size :]
+    packed_out[:, 3 * size : 4 * size] = query
+    packed_out[:, 4 * size : 5 * size] = key
+    packed_out[:, 5 * size :] = projected[:, 2 * size :]
     pre = rounded(side * scale)
     strength = jax.nn.sigmoid(pre[:, 0:1])
     mine = lax.broadcasted_iota(jnp.int32, rate_ref.shape, 1) == place
@@ -244,9 +263,9 @@
     softplus = jnp.maximum(decay, 0.0) + jnp.log(1.0 + jnp.exp(-jnp.abs(decay)))
     factor = jnp.exp(-rate * softplus)
     overlap = jnp.sum(query * key, axis=1, keepdims=True)
-    side_out[0] = jnp.broadcast_to(strength, (group_rows, size))
-    side_out[1] = jnp.broadcast_to(factor, (group_rows, size))
-    side_out[2] = jnp.broadcast_to(overlap, (group_rows, size))
+    packed_out[:, 0 * size : 1 * size] = jnp.broadcast_to(strength, (group_rows, size))
+    packed_out[:, 1 * size : 2 * size] = jnp.broadcast_to(factor, (group_rows, size))
+    packed_out[:, 2 * size : 3 * size] = jnp.broadcast_to(overlap, (group_rows, size))
     for copy in sends + core_copies + copies:
         copy.wait_send()
 
@@ -260,14 +279,18 @@
     parts = len(parts_of(cols, dims))
     extra = groups - 1
     dma = pltpu.SemaphoreType.DMA
-    vec = jax.ShapeDtypeStruct((group_rows, size), jnp.float32)
+    anywhere = pl.BlockSpec(memory_space=pl.ANY)
     return pl.pallas_call(
         functools.partial(project_kernel, heads, groups),
-        in_specs=[VMEM] * 9,
-        out_specs=[VMEM] * 5,
-        out_shape=[vec] * 4 + [jax.ShapeDtypeStruct((3, group_rows, size), jnp.float32)],
+        in_specs=[VMEM] * 2 + [anywhere] * 6 + [VMEM],
+        out_specs=VMEM,
+        out_shape=jax.ShapeDtypeStruct((group_rows, 7 * size), jnp.float32),
         scratch_shapes=[
             pltpu.VMEM((batch, cols), jnp.bfloat16),
+            pltpu.VMEM((cols, 4 * size), jnp.bfloat16),
+            pltpu.VMEM((heads, cols), jnp.bfloat16),
+            pltpu.VMEM((heads, cols), jnp.bfloat16),
+            dma((6,)),
             pltpu.VMEM((group_rows, 4 * size), jnp.float32),
             pltpu.VMEM((extra, group_rows, 4 * size), jnp.bfloat16),
             pltpu.VMEM((extra, group_rows, 4 * size), jnp.bfloat16),
@@ -290,8 +313,8 @@
         stream,
         norm_gain.reshape(groups, 1, cols),
         *weights,
-        write_weight.reshape(groups, cols, heads),
-        decay_weight.reshape(groups, cols, heads),
+        write_weight.T,
+        decay_weight.T,
         rate.reshape(1, heads),
     )
 
@@ -305,52 +328,55 @@
     count, size, _ = state_ref.shape
     key_high, key_low = split(key_ref[...])
     query_high, query_low = split(query_ref[...])
-    spots = lax.broadcasted_iota(jnp.int32, (count, size), 0)
-    recalled = jnp.zeros((count, size), jnp.float32)
-    asked = jnp.zeros((count, size), jnp.float32)
     four = jnp.concatenate([key_high, key_low, query_high, query_low], axis=0)
-    for b in range(count):
-        memory = state_ref[b].astype(jnp.bfloat16)
-        both = jnp.dot(four, memory, preferred_element_type=jnp.float32)
-        recalled = jnp.where(spots == b, both[0:count] + both[count : 2 * count], recalled)
-        asked = jnp.where(
-            spots == b, both[2 * count : 3 * count] + both[3 * count : 4 * count], asked
+    spots = lax.broadcasted_iota(jnp.int32, four.shape, 0) % count
+
+    def diagonal(rows):
+        marks = spots[0 : rows.shape[0]]
+        return jnp.concatenate(
+            [jnp.where(marks == b, rows, jnp.zeros_like(rows)) for b in range(count)], axis=1
         )
-    strength, factor, overlap = side_ref[0], side_ref[1], side_ref[2]
+
+    memory = state_ref[...].reshape(count * size, size).astype(jnp.bfloat16)
+    both = jnp.dot(diagonal(four), memory, preferred_element_type=jnp.float32)
+    recalled = both[0:count] + both[count : 2 * count]
+    asked = both[2 * count : 3 * count] + both[3 * count : 4 * count]
+    strength, factor, overlap = side_ref[:, 0:size], side_ref[:, size : 2 * size], side_ref[:, 2 * size :]
     change = strength * (value_ref[...] - factor * recalled)
     read_ref[...] = factor * asked + overlap * change
     change_high, change_low = split(change)
     left = jnp.concatenate([key_high, key_low, key_high], axis=0)
-    right = jnp.concatenate([change_high, change_high, change_low], axis=0)
-    wide_spots = lax.broadcasted_iota(jnp.int32, right.shape, 0) % count
+    left = jnp.concatenate([left, jnp.zeros((size - 3 * count, size), left.dtype)], axis=0)
+    left = left.astype(jnp.float32).T.astype(jnp.bfloat16)[:, 0 : 3 * count]
+    right = diagonal(jnp.concatenate([change_high, change_high, change_low], axis=0))
+    outer = jnp.dot(left, right, preferred_element_type=jnp.float32)
     for b in range(count):
-        only = jnp.where(wide_spots == b, right.astype(jnp.float32), 0.0).astype(jnp.bfloat16)
-        outer = lax.dot_general(
-            left, only, (((0,), (0,)), ((), ())), preferred_element_type=jnp.float32
-        )
-        new_ref[b] = factor[b : b + 1, :] * state_ref[b] + outer
-
-
-def state_step(state, query, key, value, side):
+        new_ref[b] = factor[b : b + 1, :] * state_ref[b] + outer[:, b * size : (b + 1) * size]
+
+
+def state_step(state, packed):
     count, size, _ = state.shape
     block = min(16, count)
-    row_spec = pl.BlockSpec((block, size), lambda i: (i, 0))
+
+    def columns(first, width):
+        return pl.BlockSpec((block, width), lambda i: (i, first))
+
     return pl.pallas_call(
         state_kernel,
         grid=(count // block,),
         in_specs=[
             pl.BlockSpec((block, size, size), lambda i: (i, 0, 0)),
-            row_spec,
-            row_spec,
-            row_spec,
-            pl.BlockSpec((3, block, size), lambda i: (0, i, 0)),
+            columns(4, size),
+            columns(3, size),
+            columns(5, size),
+            columns(0, 3 * size),
         ],
-        out_specs=[pl.BlockSpec((block, size, size), lambda i: (i, 0, 0)), row_spec],
+        out_specs=[pl.BlockSpec((block, size, size), lambda i: (i, 0, 0)), columns(0, size)],
         out_shape=[
             jax.ShapeDtypeStruct(state.shape, state.dtype),
             jax.ShapeDtypeStruct((count, size), jnp.float32),
         ],
-    )(state, key, query, value, side)
+    )(state, packed, packed, packed, packed)
 
 
 def output_kernel(
@@ -539,10 +565,12 @@
     heads = decay_rate.shape[0]
     groups = lax.axis_size("tp") // heads
     weights = (query_weight, key_weight, value_weight, gate_weight)
-    query, key, value, gate, side = project(
+    packed = project(
         stream, norm_gain, weights, write_weight, decay_weight, decay_rate, heads, groups
     )
-    updated, readout = state_step(state, query, key, value, side)
+    size = head_gain.shape[0]
+    updated, readout = state_step(state, packed)
+    gate = packed[:, 6 * size :]
     scaling = lax.rsqrt(jnp.mean(readout * readout, axis=1) + EPS)
     gated = (readout * head_gain.astype(jnp.float32)[None, :] * jax.nn.silu(gate)).astype(
         jnp.bfloat16

time: 94.6 us -> 92.6 us (0.979)
  local copies, waits for them, and re-layouts: 12.6 us -> 9.83 us
    unnamed x29 -> x23, local copies, waits for them, and re-layouts: 11.9 us -> 9.12 us
where the time goes in v3:
time: 92.6 us; the launch traced here: 91.8 us
  Pallas kernels  79.5 us (86%)
  local copies, waits for them, and re-layouts  9.83 us (11%)
  other arithmetic  1.8 us (2%)
    pallas_call x1, Pallas kernels, project(): pl.pallas_call(functools.partial(project_kernel, heads, groups), in_specs...  33.7 us
    pallas_call x1, Pallas kernels, output(): pl.pallas_call(functools.partial(output_kernel, heads, groups), in_specs=...  24.7 us
    pallas_call x1, Pallas kernels, state_step(): pl.pallas_call(state_kernel, grid=(count // block,), in_specs=[pl.BlockSp...  21 us
    unnamed x23, local copies, waits for them, and re-layouts  9.12 us

profile of v3, /device:TPU:0, one launch (start us, length us, event | category | flops | bytes accessed | tf_op | source)
XLA Modules:
  0.0 91.8 jit_solution(11544971666154068842)
XLA Ops:
  0.6 0.0 copy-start.1
  0.6 0.7 convert_element_type.13
  1.4 0.7 reshape.19.gain_ref
  2.1 0.0 copy-start.2
  2.1 0.9 copy-done.2
  3.0 0.0 copy-start.4
  3.0 1.0 %copy-done.4 = bf16[2048,128]{1,0:T(8,128)(2,1)S(1)} copy-done((bf16[2048,128]{1,0:T(8,128)(2,1)S(1)}, bf16[2048,128]{1,0:T(8,128)(2,1)}, u32[]{:S(2)}) %copy-start.4) | copy-done | bytes 524312
  4.0 0.0 copy-start.5
  4.0 1.0 %copy-done.5 = bf16[2048,128]{1,0:T(8,128)(2,1)S(1)} copy-done((bf16[2048,128]{1,0:T(8,128)(2,1)S(1)}, bf16[2048,128]{1,0:T(8,128)(2,1)}, u32[]{:S(2)}) %copy-start.5) | copy-done | bytes 524312
  5.1 0.0 copy-start.6
  5.1 1.0 %copy-done.6 = bf16[2048,128]{1,0:T(8,128)(2,1)S(1)} copy-done((bf16[2048,128]{1,0:T(8,128)(2,1)S(1)}, bf16[2048,128]{1,0:T(8,128)(2,1)}, u32[]{:S(2)}) %copy-start.6) | copy-done | bytes 524312
  6.1 0.0 copy-start.7
  6.1 1.0 %copy-done.7 = bf16[2048,128]{1,0:T(8,128)(2,1)S(1)} copy-done((bf16[2048,128]{1,0:T(8,128)(2,1)S(1)}, bf16[2048,128]{1,0:T(8,128)(2,1)}, u32[]{:S(2)}) %copy-start.7) | copy-done | bytes 524312
  7.1 0.0 copy-start.8
  7.1 0.9 copy-done.8
  8.0 0.0 copy-start.9
  8.0 0.9 copy-done.9
  8.9 0.0 copy-start.10
  8.9 0.7 copy-done.10
  9.6 0.0 copy-start.3
  9.6 33.7 %shard_map.131.key_ref.query_ref.value_ref.side_ref = f32[256,896]{1,0:T(8,128)S(1)} custom-call(bf16[32,2048]{1,0:T(8,128)(2,1)S(1)} %copy-done.2, bf16[2,1,2048]{2,1,0:T(2,128)(2,1)S(1)} %reshape.19.gain_ref, bf16[2048,128]{1,0:T(8,128)(2,1)S(1)} %copy-done.4, bf16[2048,128]{1,0:T(8,128)(2,1)S(1)} %copy-done.5, bf16[2048,128]{1,0:T(8,128)(2,1)S(1)} %copy-done.6, ...), custom_call_target="tpu_custom_call" | custom-call | tf_op jit(solution)/shard_map/pallas_call | solution.py:283
  43.3 0.0 copy-start
  43.3 0.9 %copy-done = f32[256,896]{1,0:T(8,128)} copy-done((f32[256,896]{1,0:T(8,128)}, f32[256,896]{1,0:T(8,128)S(1)}, u32[]{:S(2)}) %copy-start) | copy-done | bytes 917528
  44.3 21.0 %shard_map.132 = (f32[256,128,128]{2,1,0:T(8,128)}, f32[256,128]{1,0:T(8,128)}) custom-call(f32[256,128,128]{2,1,0:T(8,128)} %state_ref.1, f32[256,896]{1,0:T(8,128)} %copy-done, f32[256,896]{1,0:T(8,128)} %copy-done, f32[256,896]{1,0:T(8,128)} %copy-done, f32[256,896]{1,0:T(8,128)} %copy-done), custom_call_target="tpu_custom_call" | custom-call | tf_op jit(solution)/shard_map/pallas_call | solution.py:364
  65.3 1.1 %multiply_reduce_fusion = (f32[256]{0:T(256)S(1)}, bf16[256,128]{1,0:T(8,128)(2,1)S(1)}) fusion(f32[256,128]{1,0:T(8,128)} %get-tuple-element.4, f32[256,896]{1,0:T(8,128)} %copy-done, f32[128]{0:T(128)S(1)} %convert_element_type.13), kind=kLoop, calls=%fused_computation | loop fusion | flops 294656 | bytes 329216 | tf_op jit(solution)/shard_map/reduce_sum | solution.py:574
  66.4 0.0 copy-done.1
  66.4 0.0 copy-done.3
  66.4 24.7 %shard_map.133 = bf16[32,2048]{1,0:T(8,128)(2,1)S(1)} custom-call(bf16[32,2048]{1,0:T(8,128)(2,1)S(1)} %copy-done.3, bf16[256,128]{1,0:T(8,128)(2,1)S(1)} %get-tuple-element.7.gated_ref, bf16[16,256]{1,0:T(8,128)(2,1)S(1)} %broadcast_in_dim.2.scaling_ref, bf16[2048,128]{1,0:T(8,128)(2,1)S(1)} %copy-done.1), custom_call_target="tpu_custom_call" | custom-call | tf_op jit(solution)/shard_map/pallas_call | solution.py:522
  91.1 0.7 copy.16
  (2 shorter events, 0.0 us)
Async XLA Ops:
  0.6 65.8 %copy-start.1 = (bf16[2048,128]{1,0:T(8,128)(2,1)S(1)}, bf16[2048,128]{1,0:T(8,128)(2,1)}, u32[]{:S(2)}) copy-start(bf16[2048,128]{1,0:T(8,128)(2,1)} %weight_ref.1) | copy-start | bytes 1572868
  2.1 0.9 copy-start.2
  3.0 1.0 %copy-start.4 = (bf16[2048,128]{1,0:T(8,128)(2,1)S(1)}, bf16[2048,128]{1,0:T(8,128)(2,1)}, u32[]{:S(2)}) copy-start(bf16[2048,128]{1,0:T(8,128)(2,1)} %query_w.1) | copy-start | bytes 1572868
  4.0 1.0 %copy-start.5 = (bf16[2048,128]{1,0:T(8,128)(2,1)S(1)}, bf16[2048,128]{1,0:T(8,128)(2,1)}, u32[]{:S(2)}) copy-start(bf16[2048,128]{1,0:T(8,128)(2,1)} %key_w.1) | copy-start | bytes 1572868
  5.1 1.0 %copy-start.6 = (bf16[2048,128]{1,0:T(8,128)(2,1)S(1)}, bf16[2048,128]{1,0:T(8,128)(2,1)}, u32[]{:S(2)}) copy-start(bf16[2048,128]{1,0:T(8,128)(2,1)} %value_w.1) | copy-start | bytes 1572868
  6.1 1.0 %copy-start.7 = (bf16[2048,128]{1,0:T(8,128)(2,1)S(1)}, bf16[2048,128]{1,0:T(8,128)(2,1)}, u32[]{:S(2)}) copy-start(bf16[2048,128]{1,0:T(8,128)(2,1)} %gate_w.1) | copy-start | bytes 1572868
  7.1 0.9 copy-start.8
  8.0 0.9 copy-start.9
  8.9 0.7 copy-start.10
  9.6 56.8 %copy-start.3 = (bf16[32,2048]{1,0:T(8,128)(2,1)S(1)}, bf16[32,2048]{1,0:T(8,128)(2,1)}, u32[]{:S(2)}) copy-start(bf16[32,2048]{1,0:T(8,128)(2,1)} %stream_ref.3) | copy-start | bytes 393220
  43.3 0.9 %copy-start = (f32[256,896]{1,0:T(8,128)}, f32[256,896]{1,0:T(8,128)S(1)}, u32[]{:S(2)}) copy-start(f32[256,896]{1,0:T(8,128)S(1)} %shard_map.131.key_ref.query_ref.value_ref.side_ref) | copy-start | bytes 2752516

commit v4 on v3

--- a/solution.py
+++ b/solution.py
@@ -116,56 +116,74 @@
         fetch.start()
     enter([sibling] + neighbours + others)
 
-    def block(device_place, part):
-        (start, width), _ = part
-        begin = pl.multiple_of(device_place * rows, rows)
-        return gathered.at[pl.ds(begin, rows), pl.ds(start, width)]
-
-    parts = parts_of(cols, dims)
+    halves = 2 if rows % 32 == 0 and group_rows % rows == 0 else 1
+    part_rows = rows // halves
+    half_batch = batch // halves
+    ranges = parts_of(cols, dims)
+
+    def half_rows(h, device_place):
+        begin = h * half_batch + device_place * part_rows
+        return pl.ds(pl.multiple_of(begin, part_rows), part_rows)
+
+    def block(h, device_place, part):
+        return gathered.at[half_rows(h, device_place), pl.ds(part[0][0], part[0][1])]
+
     sends = []
-    arrivals = []
-    core_copies = []
-
-    def pass_on(p, part, bits, step):
+    core_copies = [[] for _ in range(halves)]
+
+    def pass_on(h, p, part, bits, step):
         order = part[1]
         origin = flip(place, bits)
+        target = block(h, origin, part)
         if bits:
-            source = block(origin, part)
+            source = target
         else:
-            source = stream_ref.at[:, pl.ds(part[0][0], part[0][1])]
+            source = stream_ref.at[
+                pl.ds(h * part_rows, part_rows), pl.ds(part[0][0], part[0][1])
+            ]
         for later in range(step + 1, dims):
             landed = key_of(bits + (order[later],))
             copy = remote(
                 source,
-                block(origin, part),
-                ici_send.at[p, landed],
-                ici_recv.at[p, landed],
+                target,
+                ici_send.at[h, p, landed],
+                ici_recv.at[h, p, landed],
                 flip(me, (order[later],)),
             )
             copy.start()
             sends.append(copy)
         own = key_of(bits)
-        copy = remote(
-            source, block(origin, part), core_send.at[p, own], core_recv.at[p, own], sibling
-        )
+        copy = remote(source, target, core_send.at[h, p, own], core_recv.at[h, p, own], sibling)
         copy.start()
-        core_copies.append(copy)
-
-    def arrived(p, part, bits):
-        landed = key_of(bits)
-        target = block(flip(place, bits), part)
-        remote(target, target, ici_send.at[p, landed], ici_recv.at[p, landed], sibling).wait_recv()
-
-    for p, part in enumerate(parts):
-        pass_on(p, part, (), -1)
-    own_rows = pl.ds(pl.multiple_of(place * rows, rows), rows)
-    gathered[own_rows, :] = stream_ref[...]
-    for index in range(1, 1 << dims):
-        for p, part in enumerate(parts):
+        core_copies[h].append(copy)
+
+    def begin(h):
+        for p, part in enumerate(ranges):
+            pass_on(h, p, part, (), -1)
+
+    def relay(h, index):
+        for p, part in enumerate(ranges):
             bits, step = masks_of(part[1])[index]
-            arrived(p, part, bits)
-            pass_on(p, part, bits, step)
-    for copy in core_copies:
+            landed = key_of(bits)
+            target = block(h, flip(place, bits), part)
+            remote(
+                target, target, ici_send.at[h, p, landed], ici_recv.at[h, p, landed], sibling
+            ).wait_recv()
+            pass_on(h, p, part, bits, step)
+
+    early = max(2, 1 << (dims - 1))
+    begin(0)
+    for h in range(halves):
+        gathered[half_rows(h, place), :] = stream_ref[h * part_rows : (h + 1) * part_rows, :]
+    relay(0, 1)
+    for h in range(1, halves):
+        begin(h)
+    for index in range(2, 1 << dims):
+        relay(0, index)
+    for h in range(1, halves):
+        for index in range(1, early):
+            relay(h, index)
+    for copy in core_copies[0]:
         copy.wait_recv()
 
     gain = gain_ref[group].astype(jnp.float32)
@@ -204,30 +222,43 @@
 
     copies = []
     wide = max(group_rows, 128)
-    for j in list(range(1, groups)) + [0]:
-        target_group = (group + j) % groups
-        begin = pl.multiple_of(target_group * group_rows, group_rows)
-        side = project(begin, group_rows, 0)
-        if j:
-            sent[j - 1] = partial[...].astype(jnp.bfloat16)
-            turned[0:group_rows, :] = side
+    count = group_rows // halves
+
+    def half_of(h, target_group):
+        begin = h * half_batch + target_group * count
+        return pl.multiple_of(begin, count)
+
+    for h in range(halves):
+        if h:
+            for index in range(early, 1 << dims):
+                relay(h, index)
+            for copy in core_copies[h]:
+                copy.wait_recv()
+        for j in range(1, groups):
+            spot = slice(h * count, (h + 1) * count)
+            side = project(half_of(h, (group + j) % groups), count, 0)
+            sent[j - 1, spot] = partial[0:count].astype(jnp.bfloat16)
+            turned[spot] = side
+            routes = [(sent.at[j - 1, spot], received.at[j - 1, spot], group_send, group_recv)]
             flat = turned[...].T
-            small_sent[j - 1] = flat[0:SMALL, 0:group_rows].astype(jnp.bfloat16)
-            for source, target, send, recv in (
-                (sent, received, group_send, group_recv),
-                (small_sent, small_received, small_send, small_recv),
-            ):
+            small_sent[j - 1, :, spot] = flat[0:SMALL, spot].astype(jnp.bfloat16)
+            routes.append(
+                (
+                    small_sent.at[j - 1, :, spot],
+                    small_received.at[j - 1, :, spot],
+                    small_send,
+                    small_recv,
+                )
+            )
+            for source, target, send, recv in routes:
                 copy = remote(
-                    source.at[j - 1],
-                    target.at[j - 1],
-                    send.at[j - 1],
-                    recv.at[j - 1],
-                    others[j - 1],
+                    source, target, send.at[h, j - 1], recv.at[h, j - 1], others[j - 1]
                 )
                 copy.start()
                 copies.append(copy)
+    for h in range(halves):
+        turned[h * count : (h + 1) * count] = project(half_of(h, group), count, h * count)
     total = partial[...]
-    turned[0:group_rows, :] = side
     flat = turned[...].T[0:SMALL, :]
     for copy in copies:
         copy.wait_recv()
@@ -252,9 +283,6 @@
     key = projected[:, size : 2 * size]
     query = query * lax.rsqrt(jnp.sum(query * query, axis=1, keepdims=True) + EPS) * size**-0.5
     key = key * lax.rsqrt(jnp.sum(key * key, axis=1, keepdims=True) + EPS)
-    packed_out[:, 3 * size : 4 * size] = query
-    packed_out[:, 4 * size : 5 * size] = key
-    packed_out[:, 5 * size :] = projected[:, 2 * size :]
     pre = rounded(side * scale)
     strength = jax.nn.sigmoid(pre[:, 0:1])
     mine = lax.broadcasted_iota(jnp.int32, rate_ref.shape, 1) == place
@@ -263,10 +291,18 @@
     softplus = jnp.maximum(decay, 0.0) + jnp.log(1.0 + jnp.exp(-jnp.abs(decay)))
     factor = jnp.exp(-rate * softplus)
     overlap = jnp.sum(query * key, axis=1, keepdims=True)
-    packed_out[:, 0 * size : 1 * size] = jnp.broadcast_to(strength, (group_rows, size))
-    packed_out[:, 1 * size : 2 * size] = jnp.broadcast_to(factor, (group_rows, size))
-    packed_out[:, 2 * size : 3 * size] = jnp.broadcast_to(overlap, (group_rows, size))
-    for copy in sends + core_copies + copies:
+    results = [jnp.broadcast_to(v, (group_rows, size)) for v in (strength, factor, overlap)]
+    results += [query, key, projected[:, 2 * size :]]
+    for i, v in enumerate(results):
+        span = pl.ds(i * size, v.shape[1])
+        if halves == 1:
+            packed_out[:, span] = v
+            continue
+        for h in range(halves):
+            for q in range(group_rows // rows):
+                to, come = q * rows + h * part_rows, h * count + q * part_rows
+                packed_out[to : to + part_rows, span] = v[come : come + part_rows]
+    for copy in sends + sum(core_copies, []) + copies:
         copy.wait_send()
 
 
@@ -278,6 +314,7 @@
     dims = heads.bit_length() - 2
     parts = len(parts_of(cols, dims))
     extra = groups - 1
+    halves = 2
     dma = pltpu.SemaphoreType.DMA
     anywhere = pl.BlockSpec(memory_space=pl.ANY)
     return pl.pallas_call(
@@ -297,17 +334,17 @@
             pltpu.VMEM((extra, SMALL, group_rows), jnp.bfloat16),
             pltpu.VMEM((extra, SMALL, group_rows), jnp.bfloat16),
             pltpu.VMEM((max(group_rows, 128), 128), jnp.float32),
-            dma((parts, 1 << dims)),
-            dma((parts, 1 << dims)),
-            dma((parts, 1 << dims)),
-            dma((parts, 1 << dims)),
-            dma((extra,)),
-            dma((extra,)),
-            dma((extra,)),
-            dma((extra,)),
+            dma((halves, parts, 1 << dims)),
+            dma((halves, parts, 1 << dims)),
+            dma((halves, parts, 1 << dims)),
+            dma((halves, parts, 1 << dims)),
+            dma((halves, extra)),
+            dma((halves, extra)),
+            dma((halves, extra)),
+            dma((halves, extra)),
         ],
         compiler_params=pltpu.CompilerParams(
-            collective_id=0, has_side_effects=True, vmem_limit_bytes=48 * 1024 * 1024
+            collective_id=0, has_side_effects=True
         ),
     )(
         stream,
@@ -324,12 +361,27 @@
     return high, (v - high.astype(jnp.float32)).astype(jnp.bfloat16)
 
 
-def state_kernel(state_ref, key_ref, query_ref, value_ref, side_ref, new_ref, read_ref):
-    count, size, _ = state_ref.shape
-    key_high, key_low = split(key_ref[...])
-    query_high, query_low = split(query_ref[...])
-    four = jnp.concatenate([key_high, key_low, query_high, query_low], axis=0)
-    spots = lax.broadcasted_iota(jnp.int32, four.shape, 0) % count
+def state_kernel(
+    state_ref, packed_ref, gain_ref, new_ref, gated_ref, flat_ref, held, readout, in_sems, out_sems
+):
+    total, size, _ = state_ref.shape
+    steps = in_sems.shape[0]
+    count = total // steps
+
+    def rows_of(step):
+        return pl.ds(pl.multiple_of(step * count, count), count)
+
+    def fetch(step):
+        rows = rows_of(step)
+        return pltpu.make_async_copy(state_ref.at[rows], held.at[rows], in_sems.at[step])
+
+    def store(step):
+        rows = rows_of(step)
+        return pltpu.make_async_copy(held.at[rows], new_ref.at[rows], out_sems.at[step])
+
+    for step in range(steps):
+        fetch(step).start()
+    spots = lax.broadcasted_iota(jnp.int32, (4 * count, size), 0) % count
 
     def diagonal(rows):
         marks = spots[0 : rows.shape[0]]
@@ -337,46 +389,71 @@
             [jnp.where(marks == b, rows, jnp.zeros_like(rows)) for b in range(count)], axis=1
         )
 
-    memory = state_ref[...].reshape(count * size, size).astype(jnp.bfloat16)
-    both = jnp.dot(diagonal(four), memory, preferred_element_type=jnp.float32)
-    recalled = both[0:count] + both[count : 2 * count]
-    asked = both[2 * count : 3 * count] + both[3 * count : 4 * count]
-    strength, factor, overlap = side_ref[:, 0:size], side_ref[:, size : 2 * size], side_ref[:, 2 * size :]
-    change = strength * (value_ref[...] - factor * recalled)
-    read_ref[...] = factor * asked + overlap * change
-    change_high, change_low = split(change)
-    left = jnp.concatenate([key_high, key_low, key_high], axis=0)
-    left = jnp.concatenate([left, jnp.zeros((size - 3 * count, size), left.dtype)], axis=0)
-    left = left.astype(jnp.float32).T.astype(jnp.bfloat16)[:, 0 : 3 * count]
-    right = diagonal(jnp.concatenate([change_high, change_high, change_low], axis=0))
-    outer = jnp.dot(left, right, preferred_element_type=jnp.float32)
-    for b in range(count):
-        new_ref[b] = factor[b : b + 1, :] * state_ref[b] + outer[:, b * size : (b + 1) * size]
-
-
-def state_step(state, packed):
+    def body(step, carry):
+        rows = rows_of(step)
+
+        def columns(first, width=1):
+            return packed_ref[rows, first * size : (first + width) * size]
+
+        key_high, key_low = split(columns(4))
+        query_high, query_low = split(columns(3))
+        four = jnp.concatenate([key_high, key_low, query_high, query_low], axis=0)
+        strength, factor, overlap = columns(0), columns(1), columns(2)
+        left = jnp.concatenate([key_high, key_low, key_high], axis=0)
+        left = jnp.concatenate([left, jnp.zeros((size - 3 * count, size), left.dtype)], axis=0)
+        left = left.astype(jnp.float32).T.astype(jnp.bfloat16)[:, 0 : 3 * count]
+        wide = diagonal(four)
+        fetch(step).wait()
+        memory = held[rows].reshape(count * size, size).astype(jnp.bfloat16)
+        both = jnp.dot(wide, memory, preferred_element_type=jnp.float32)
+        recalled = both[0:count] + both[count : 2 * count]
+        asked = both[2 * count : 3 * count] + both[3 * count : 4 * count]
+        change = strength * (columns(5) - factor * recalled)
+        readout[rows, :] = factor * asked + overlap * change
+        change_high, change_low = split(change)
+        right = diagonal(jnp.concatenate([change_high, change_high, change_low], axis=0))
+        outer = jnp.dot(left, right, preferred_element_type=jnp.float32)
+        for b in range(count):
+            spot = step * count + b
+            held[spot] = factor[b : b + 1, :] * held[spot] + outer[:, b * size : (b + 1) * size]
+        store(step).start()
+        return carry
+
+    lax.fori_loop(0, steps, body, 0)
+    read = readout[...]
+    scaling = lax.rsqrt(jnp.sum(read * read, axis=1, keepdims=True) / size + EPS)
+    gate = packed_ref[:, 6 * size :]
+    gated_ref[...] = (
+        read * gain_ref[...].astype(jnp.float32) * (gate / (1.0 + jnp.exp(-gate)))
+    ).astype(jnp.bfloat16)
+    tall = jnp.broadcast_to(scaling, (total, 128))
+    if total < 128:
+        tall = jnp.concatenate([tall, jnp.zeros((128 - total, 128), jnp.float32)], axis=0)
+    flat_ref[...] = tall.T[0:SMALL, 0:total].astype(jnp.bfloat16)
+    for step in range(steps):
+        store(step).wait()
+
+
+def state_step(state, packed, head_gain):
     count, size, _ = state.shape
-    block = min(16, count)
-
-    def columns(first, width):
-        return pl.BlockSpec((block, width), lambda i: (i, first))
-
+    steps = count // min(16, count)
+    anywhere = pl.BlockSpec(memory_space=pl.ANY)
     return pl.pallas_call(
         state_kernel,
-        grid=(count // block,),
-        in_specs=[
-            pl.BlockSpec((block, size, size), lambda i: (i, 0, 0)),
-            columns(4, size),
-            columns(3, size),
-            columns(5, size),
-            columns(0, 3 * size),
-        ],
-        out_specs=[pl.BlockSpec((block, size, size), lambda i: (i, 0, 0)), columns(0, size)],
+        in_specs=[anywhere, VMEM, VMEM],
+        out_specs=[anywhere, VMEM, VMEM],
         out_shape=[
             jax.ShapeDtypeStruct(state.shape, state.dtype),
-            jax.ShapeDtypeStruct((count, size), jnp.float32),
+            jax.ShapeDtypeStruct((count, size), jnp.bfloat16),
+            jax.ShapeDtypeStruct((SMALL, count), jnp.bfloat16),
         ],
-    )(state, packed, packed, packed, packed)
+        scratch_shapes=[
+            pltpu.VMEM(state.shape, state.dtype),
+            pltpu.VMEM((count, size), jnp.float32),
+            pltpu.SemaphoreType.DMA((steps,)),
+            pltpu.SemaphoreType.DMA((steps,)),
+        ],
+    )(state, packed, head_gain.reshape(1, size))
 
 
 def output_kernel(
@@ -385,8 +462,10 @@
     stream_ref,
     gated_ref,
     scaling_ref,
+    weight_hbm,
+    out_ref,
     weight_ref,
-    out_ref,
+    weight_sem,
     all_gated,
     all_scaling,
     columns,
@@ -415,6 +494,8 @@
     sibling = flip(me, (0,))
     neighbours = [flip(me, (bit,)) for bit in range(1, dims + 1)]
     others = [place + heads * ((group + j) % groups) for j in range(1, groups)]
+    weight_copy = pltpu.make_async_copy(weight_hbm, weight_ref, weight_sem)
+    weight_copy.start()
     enter([sibling] + neighbours + others)
     own_rows = pl.ds(pl.multiple_of(group * group_rows, group_rows), group_rows)
     copies = []
@@ -431,6 +512,7 @@
     all_scaling[group] = scaling_ref[...]
     for copy in copies:
         copy.wait_recv()
+    weight_copy.wait()
     wide = max(group_rows, 128)
     for g in range(groups):
         flat = all_scaling[g].astype(jnp.float32)
@@ -518,13 +600,15 @@
     parts = len(parts_of(cols, dims))
     extra = groups - 1
     dma = pltpu.SemaphoreType.DMA
-    flat = jnp.broadcast_to(scaling.astype(jnp.bfloat16)[None, :], (SMALL, group_rows))
+    anywhere = pl.BlockSpec(memory_space=pl.ANY)
     return pl.pallas_call(
         functools.partial(output_kernel, heads, groups),
-        in_specs=[VMEM] * 4,
+        in_specs=[VMEM] * 3 + [anywhere],
         out_specs=VMEM,
         out_shape=jax.ShapeDtypeStruct(stream.shape, stream.dtype),
         scratch_shapes=[
+            pltpu.VMEM(out_weight.shape, out_weight.dtype),
+            dma(()),
             pltpu.VMEM((batch, size), jnp.bfloat16),
             pltpu.VMEM((groups, SMALL, group_rows), jnp.bfloat16),
             pltpu.VMEM((batch, 128), jnp.float32),
@@ -543,9 +627,9 @@
             dma((dims, parts, chips)),
         ],
         compiler_params=pltpu.CompilerParams(
-            collective_id=1, has_side_effects=True, vmem_limit_bytes=48 * 1024 * 1024
+            collective_id=1, has_side_effects=True
         ),
-    )(stream, gated, flat, out_weight)
+    )(stream, gated, scaling, out_weight)
 
 
 def per_device(
@@ -568,13 +652,7 @@
     packed = project(
         stream, norm_gain, weights, write_weight, decay_weight, decay_rate, heads, groups
     )
-    size = head_gain.shape[0]
-    updated, readout = state_step(state, packed)
-    gate = packed[:, 6 * size :]
-    scaling = lax.rsqrt(jnp.mean(readout * readout, axis=1) + EPS)
-    gated = (readout * head_gain.astype(jnp.float32)[None, :] * jax.nn.silu(gate)).astype(
-        jnp.bfloat16
-    )
+    updated, gated, scaling = state_step(state, packed, head_gain)
     result = output(stream, gated, scaling, out_weight, heads, groups)
     return (result, updated)
 

time: 92.6 us -> 78.4 us (0.85)
  local copies, waits for them, and re-layouts: 9.83 us -> 2.88 us
  Pallas kernels: 79.5 us -> 74.7 us
  other arithmetic: 1.8 us -> 0 us
    unnamed x23 -> x1, local copies, waits for them, and re-layouts: 9.12 us -> 1.57 us
    pallas_call x1, Pallas kernels: 21 us -> 14.1 us  [state_step(): pl.pallas_call(state_kernel, in_specs=[anywhere, VMEM, VMEM], out_specs=[...]
    pallas_call x1, Pallas kernels: 24.7 us -> 26.2 us  [output(): pl.pallas_call(functools.partial(output_kernel, heads, groups), in_specs=...]
    reduce_sum x1 -> x0, other arithmetic: 1.08 us -> none  [per_device(): scaling = lax.rsqrt(jnp.mean(readout * readout, axis=1) + EPS)]
where the time goes in v4:
time: 78.4 us; the launch traced here: 78.2 us
  Pallas kernels  74.7 us (95%)
  local copies, waits for them, and re-layouts  2.88 us (4%)
    pallas_call x1, Pallas kernels, project(): pl.pallas_call(functools.partial(project_kernel, heads, groups), in_specs...  34.4 us
    pallas_call x1, Pallas kernels, output(): pl.pallas_call(functools.partial(output_kernel, heads, groups), in_specs=...  26.2 us
    pallas_call x1, Pallas kernels, state_step(): pl.pallas_call(state_kernel, in_specs=[anywhere, VMEM, VMEM], out_specs=[...  14.1 us
    unnamed x1, local copies, waits for them, and re-layouts  1.57 us

profile of v4, /device:TPU:0, one launch (start us, length us, event | category | flops | bytes accessed | tf_op | source)
XLA Modules:
  0.0 78.2 jit_solution(8268147872411369959)
XLA Ops:
  0.6 1.3 %reshape.16.gain_ref = bf16[2,1,2048]{2,1,0:T(2,128)(2,1)} reshape(bf16[4096]{0:T(1024)(128)(2,1)} %param.13) | data formatting | bytes 16384 | tf_op jit(solution)/shard_map/reshape | solution.py:351
  1.9 34.4 %shard_map.131.packed_ref = f32[256,896]{1,0:T(8,128)} custom-call(bf16[32,2048]{1,0:T(8,128)(2,1)} %stream_ref.3, bf16[2,1,2048]{2,1,0:T(2,128)(2,1)} %reshape.16.gain_ref, bf16[2048,128]{1,0:T(8,128)(2,1)} %query_w.1, bf16[2048,128]{1,0:T(8,128)(2,1)} %key_w.1, bf16[2048,128]{1,0:T(8,128)(2,1)} %value_w.1, bf16[2048,128]{1,0:T(8,128)(2,1)} %gate_w.1, ...), custom_call_target="tpu_custom_call" | custom-call | tf_op jit(solution)/shard_map/pallas_call | solution.py:320
  36.3 14.1 %shard_map.132 = (f32[256,128,128]{2,1,0:T(8,128)}, bf16[256,128]{1,0:T(8,128)(2,1)}, bf16[16,256]{1,0:T(8,128)(2,1)}) custom-call(f32[256,128,128]{2,1,0:T(8,128)} %state_ref.1, f32[256,896]{1,0:T(8,128)} %shard_map.131.packed_ref, bf16[1,128]{1,0:T(2,128)(2,1)} %bitcast.6), custom_call_target="tpu_custom_call" | custom-call | tf_op jit(solution)/shard_map/pallas_call | solution.py:441
  50.4 26.2 %shard_map.133 = bf16[32,2048]{1,0:T(8,128)(2,1)} custom-call(bf16[32,2048]{1,0:T(8,128)(2,1)} %stream_ref.3, bf16[256,128]{1,0:T(8,128)(2,1)} %get-tuple-element.5.gated_ref, bf16[16,256]{1,0:T(8,128)(2,1)} %get-tuple-element.6.scaling_ref, bf16[2048,128]{1,0:T(8,128)(2,1)} %weight_hbm.1), custom_call_target="tpu_custom_call" | custom-call | tf_op jit(solution)/shard_map/pallas_call | solution.py:604
  76.6 1.6 %copy.16 = bf16[32,2048]{1,0:T(8,128)(2,1)} copy(bf16[32,2048]{1,0:T(8,128)(2,1)} %shard_map.133) | data formatting | bytes 262144

commit v5 on v4

--- a/solution.py
+++ b/solution.py
@@ -556,36 +556,39 @@
         product = head_rows(place, masks)
         for i, mask in enumerate(masks):
             held[mask] = product[i * rows : (i + 1) * rows]
+
+    parts = parts_of(cols, dims)
+    hops = []
+    waiting = [[] for _ in range(dims)]
+
+    def cross(step, p, mask):
+        (start, width), order = parts[p]
+        if step == dims or not mask >> (order[step] - 1) & 1:
+            return
+        span = pl.ds(start, width)
+        landed = mask - (1 << (order[step] - 1))
+        hop_out[step, landed, :, span] = held[mask, :, span].astype(jnp.bfloat16)
+        copy = remote(
+            hop_out.at[step, landed, :, span],
+            hop_in.at[step, landed, :, span],
+            hop_send.at[step, p, landed],
+            hop_recv.at[step, p, landed],
+            neighbours[order[step] - 1],
+        )
+        copy.start()
+        hops.append(copy)
+        waiting[step].append((p, landed, span, copy))
+
     for mask in sweep:
         core_copies[mask].wait_recv()
         held[mask] += core_in[mask].astype(jnp.float32)
-
-    parts = parts_of(cols, dims)
-    hops = []
+        for p in range(len(parts)):
+            cross(0, p, mask)
     for step in range(dims):
-        started = []
-        for p, ((start, width), order) in enumerate(parts):
-            span = pl.ds(start, width)
-            crossed = [1 << (bit - 1) for bit in order[:step]]
-            now = 1 << (order[step] - 1)
-            for mask in range(chips):
-                if any(mask & c for c in crossed) or not mask & now:
-                    continue
-                landed = mask - now
-                hop_out[step, landed, :, span] = held[mask, :, span].astype(jnp.bfloat16)
-                copy = remote(
-                    hop_out.at[step, landed, :, span],
-                    hop_in.at[step, landed, :, span],
-                    hop_send.at[step, p, landed],
-                    hop_recv.at[step, p, landed],
-                    neighbours[order[step] - 1],
-                )
-                copy.start()
-                started.append((landed, span, copy))
-        for landed, span, copy in started:
+        for p, landed, span, copy in waiting[step]:
             copy.wait_recv()
             held[landed, :, span] += hop_in[step, landed, :, span].astype(jnp.float32)
-            hops.append(copy)
+            cross(step + 1, p, landed)
     out_ref[...] = (stream_ref[...].astype(jnp.float32) + held[0]).astype(jnp.bfloat16)
     for copy in copies + core_copies + hops:
         copy.wait_send()

time: 78.4 us -> 73.5 us (0.937)
  Pallas kernels: 74.7 us -> 69.8 us
    pallas_call x1, Pallas kernels: 26.2 us -> 21.3 us  [output(): pl.pallas_call(functools.partial(output_kernel, heads, groups), in_specs=...]
where the time goes in v5:
time: 73.5 us; the launch traced here: 73.3 us
  Pallas kernels  69.8 us (95%)
  local copies, waits for them, and re-layouts  2.88 us (4%)
    pallas_call x1, Pallas kernels, project(): pl.pallas_call(functools.partial(project_kernel, heads, groups), in_specs...  34.4 us
    pallas_call x1, Pallas kernels, output(): pl.pallas_call(functools.partial(output_kernel, heads, groups), in_specs=...  21.3 us
    pallas_call x1, Pallas kernels, state_step(): pl.pallas_call(state_kernel, in_specs=[anywhere, VMEM, VMEM], out_specs=[...  14.1 us
    unnamed x1, local copies, waits for them, and re-layouts  1.57 us

profile of v5, /device:TPU:0, one launch (start us, length us, event | category | flops | bytes accessed | tf_op | source)
XLA Modules:
  0.0 73.3 jit_solution(9893591749644444268)
XLA Ops:
  0.6 1.3 %reshape.16.gain_ref = bf16[2,1,2048]{2,1,0:T(2,128)(2,1)} reshape(bf16[4096]{0:T(1024)(128)(2,1)} %param.13) | data formatting | bytes 16384 | tf_op jit(solution)/shard_map/reshape | solution.py:351
  1.9 34.4 %shard_map.131.packed_ref = f32[256,896]{1,0:T(8,128)} custom-call(bf16[32,2048]{1,0:T(8,128)(2,1)} %stream_ref.3, bf16[2,1,2048]{2,1,0:T(2,128)(2,1)} %reshape.16.gain_ref, bf16[2048,128]{1,0:T(8,128)(2,1)} %query_w.1, bf16[2048,128]{1,0:T(8,128)(2,1)} %key_w.1, bf16[2048,128]{1,0:T(8,128)(2,1)} %value_w.1, bf16[2048,128]{1,0:T(8,128)(2,1)} %gate_w.1, ...), custom_call_target="tpu_custom_call" | custom-call | tf_op jit(solution)/shard_map/pallas_call | solution.py:320
  36.3 14.1 %shard_map.132 = (f32[256,128,128]{2,1,0:T(8,128)}, bf16[256,128]{1,0:T(8,128)(2,1)}, bf16[16,256]{1,0:T(8,128)(2,1)}) custom-call(f32[256,128,128]{2,1,0:T(8,128)} %state_ref.1, f32[256,896]{1,0:T(8,128)} %shard_map.131.packed_ref, bf16[1,128]{1,0:T(2,128)(2,1)} %bitcast.6), custom_call_target="tpu_custom_call" | custom-call | tf_op jit(solution)/shard_map/pallas_call | solution.py:441
  50.4 21.3 %shard_map.133 = bf16[32,2048]{1,0:T(8,128)(2,1)} custom-call(bf16[32,2048]{1,0:T(8,128)(2,1)} %stream_ref.3, bf16[256,128]{1,0:T(8,128)(2,1)} %get-tuple-element.5.gated_ref, bf16[16,256]{1,0:T(8,128)(2,1)} %get-tuple-element.6.scaling_ref, bf16[2048,128]{1,0:T(8,128)(2,1)} %weight_hbm.1), custom_call_target="tpu_custom_call" | custom-call | tf_op jit(solution)/shard_map/pallas_call | solution.py:607
  71.7 1.6 %copy.16 = bf16[32,2048]{1,0:T(8,128)(2,1)} copy(bf16[32,2048]{1,0:T(8,128)(2,1)} %shard_map.133) | data formatting | bytes 262144

commit v6 on v5

--- a/solution.py
+++ b/solution.py
@@ -75,6 +75,7 @@
     weights,
     write_t,
     decay_t,
+    gains,
     local_sems,
     partial,
     sent,
@@ -171,7 +172,7 @@
             ).wait_recv()
             pass_on(h, p, part, bits, step)
 
-    early = max(2, 1 << (dims - 1))
+    early = 1
     begin(0)
     for h in range(halves):
         gathered[half_rows(h, place), :] = stream_ref[h * part_rows : (h + 1) * part_rows, :]
@@ -186,7 +187,10 @@
     for copy in core_copies[0]:
         copy.wait_recv()
 
-    gain = gain_ref[group].astype(jnp.float32)
+    gains[...] = gain_ref[...].astype(jnp.float32)
+    gain = jnp.concatenate(
+        [gains[pl.ds(group * (cols // 128) + i, 1), :] for i in range(cols // 128)], axis=1
+    )
     for fetch in fetches:
         fetch.wait()
 
@@ -327,6 +331,7 @@
             pltpu.VMEM((cols, 4 * size), jnp.bfloat16),
             pltpu.VMEM((heads, cols), jnp.bfloat16),
             pltpu.VMEM((heads, cols), jnp.bfloat16),
+            pltpu.VMEM((groups * cols // 128, 128), jnp.float32),
             dma((6,)),
             pltpu.VMEM((group_rows, 4 * size), jnp.float32),
             pltpu.VMEM((extra, group_rows, 4 * size), jnp.bfloat16),
@@ -348,7 +353,7 @@
         ),
     )(
         stream,
-        norm_gain.reshape(groups, 1, cols),
+        norm_gain.reshape(groups * cols // 128, 128),
         *weights,
         write_weight.T,
         decay_weight.T,

time: 73.5 us -> 74.5 us (1.014)
  Pallas kernels: 69.8 us -> 72.1 us
  local copies, waits for them, and re-layouts: 2.88 us -> 1.57 us
    pallas_call x1, Pallas kernels: 34.4 us -> 35.9 us  [project(): pl.pallas_call(functools.partial(project_kernel, heads, groups), in_specs...]
    reshape x1 -> x0, local copies, waits for them, and re-layouts: 1.31 us -> none  [project(): norm_gain.reshape(groups, 1, cols)]
    pallas_call x1, Pallas kernels: 21.3 us -> 22.1 us  [output(): pl.pallas_call(functools.partial(output_kernel, heads, groups), in_specs=...]
where the time goes in v6:
time: 74.5 us; the launch traced here: 74.3 us
  Pallas kernels  72.1 us (97%)
  local copies, waits for them, and re-layouts  1.57 us (2%)
    pallas_call x1, Pallas kernels, project(): pl.pallas_call(functools.partial(project_kernel, heads, groups), in_specs...  35.9 us
    pallas_call x1, Pallas kernels, output(): pl.pallas_call(functools.partial(output_kernel, heads, groups), in_specs=...  22.1 us
    pallas_call x1, Pallas kernels, state_step(): pl.pallas_call(state_kernel, in_specs=[anywhere, VMEM, VMEM], out_specs=[...  14.1 us
    unnamed x1, local copies, waits for them, and re-layouts  1.57 us

profile of v6, /device:TPU:0, one launch (start us, length us, event | category | flops | bytes accessed | tf_op | source)
XLA Modules:
  0.0 74.3 jit_solution(2211564892933461453)
XLA Ops:
  0.6 35.9 %shard_map.131.packed_ref = f32[256,896]{1,0:T(8,128)} custom-call(bf16[32,2048]{1,0:T(8,128)(2,1)} %stream_ref.3, bf16[32,128]{1,0:T(8,128)(2,1)} %bitcast.7, bf16[2048,128]{1,0:T(8,128)(2,1)} %query_w.1, bf16[2048,128]{1,0:T(8,128)(2,1)} %key_w.1, bf16[2048,128]{1,0:T(8,128)(2,1)} %value_w.1, bf16[2048,128]{1,0:T(8,128)(2,1)} %gate_w.1, ...), custom_call_target="tpu_custom_call" | custom-call | tf_op jit(solution)/shard_map/pallas_call | solution.py:324
  36.5 14.1 %shard_map.132 = (f32[256,128,128]{2,1,0:T(8,128)}, bf16[256,128]{1,0:T(8,128)(2,1)}, bf16[16,256]{1,0:T(8,128)(2,1)}) custom-call(f32[256,128,128]{2,1,0:T(8,128)} %state_ref.1, f32[256,896]{1,0:T(8,128)} %shard_map.131.packed_ref, bf16[1,128]{1,0:T(2,128)(2,1)} %bitcast.8), custom_call_target="tpu_custom_call" | custom-call | tf_op jit(solution)/shard_map/pallas_call | solution.py:446
  50.7 22.1 %shard_map.133 = bf16[32,2048]{1,0:T(8,128)(2,1)} custom-call(bf16[32,2048]{1,0:T(8,128)(2,1)} %stream_ref.3, bf16[256,128]{1,0:T(8,128)(2,1)} %get-tuple-element.5.gated_ref, bf16[16,256]{1,0:T(8,128)(2,1)} %get-tuple-element.6.scaling_ref, bf16[2048,128]{1,0:T(8,128)(2,1)} %weight_hbm.1), custom_call_target="tpu_custom_call" | custom-call | tf_op jit(solution)/shard_map/pallas_call | solution.py:612
  72.7 1.6 %copy.15 = bf16[32,2048]{1,0:T(8,128)(2,1)} copy(bf16[32,2048]{1,0:T(8,128)(2,1)} %shard_map.133) | data formatting | bytes 262144

commit v7 on v6

--- a/solution.py
+++ b/solution.py
@@ -172,7 +172,7 @@
             ).wait_recv()
             pass_on(h, p, part, bits, step)
 
-    early = 1
+    early = max(2, 1 << (dims - 1))
     begin(0)
     for h in range(halves):
         gathered[half_rows(h, place), :] = stream_ref[h * part_rows : (h + 1) * part_rows, :]

time: 74.5 us -> 72.2 us (0.969)
  Pallas kernels: 72.1 us -> 69.8 us
    pallas_call x1, Pallas kernels: 35.9 us -> 34.4 us  [project(): pl.pallas_call(functools.partial(project_kernel, heads, groups), in_specs...]
    pallas_call x1, Pallas kernels: 22.1 us -> 21.3 us  [output(): pl.pallas_call(functools.partial(output_kernel, heads, groups), in_specs=...]
where the time goes in v7:
time: 72.2 us; the launch traced here: 72 us
  Pallas kernels  69.8 us (97%)
  local copies, waits for them, and re-layouts  1.57 us (2%)
    pallas_call x1, Pallas kernels, project(): pl.pallas_call(functools.partial(project_kernel, heads, groups), in_specs...  34.4 us
    pallas_call x1, Pallas kernels, output(): pl.pallas_call(functools.partial(output_kernel, heads, groups), in_specs=...  21.3 us
    pallas_call x1, Pallas kernels, state_step(): pl.pallas_call(state_kernel, in_specs=[anywhere, VMEM, VMEM], out_specs=[...  14.1 us
    unnamed x1, local copies, waits for them, and re-layouts  1.57 us

profile of v7, /device:TPU:0, one launch (start us, length us, event | category | flops | bytes accessed | tf_op | source)
XLA Modules:
  0.0 72.0 jit_solution(2765257124837227131)
XLA Ops:
  0.6 34.4 %shard_map.131.packed_ref = f32[256,896]{1,0:T(8,128)} custom-call(bf16[32,2048]{1,0:T(8,128)(2,1)} %stream_ref.3, bf16[32,128]{1,0:T(8,128)(2,1)} %bitcast.7, bf16[2048,128]{1,0:T(8,128)(2,1)} %query_w.1, bf16[2048,128]{1,0:T(8,128)(2,1)} %key_w.1, bf16[2048,128]{1,0:T(8,128)(2,1)} %value_w.1, bf16[2048,128]{1,0:T(8,128)(2,1)} %gate_w.1, ...), custom_call_target="tpu_custom_call" | custom-call | tf_op jit(solution)/shard_map/pallas_call | solution.py:324
  35.0 14.1 %shard_map.132 = (f32[256,128,128]{2,1,0:T(8,128)}, bf16[256,128]{1,0:T(8,128)(2,1)}, bf16[16,256]{1,0:T(8,128)(2,1)}) custom-call(f32[256,128,128]{2,1,0:T(8,128)} %state_ref.1, f32[256,896]{1,0:T(8,128)} %shard_map.131.packed_ref, bf16[1,128]{1,0:T(2,128)(2,1)} %bitcast.8), custom_call_target="tpu_custom_call" | custom-call | tf_op jit(solution)/shard_map/pallas_call | solution.py:446
  49.1 21.3 %shard_map.133 = bf16[32,2048]{1,0:T(8,128)(2,1)} custom-call(bf16[32,2048]{1,0:T(8,128)(2,1)} %stream_ref.3, bf16[256,128]{1,0:T(8,128)(2,1)} %get-tuple-element.5.gated_ref, bf16[16,256]{1,0:T(8,128)(2,1)} %get-tuple-element.6.scaling_ref, bf16[2048,128]{1,0:T(8,128)(2,1)} %weight_hbm.1), custom_call_target="tpu_custom_call" | custom-call | tf_op jit(solution)/shard_map/pallas_call | solution.py:612
  70.4 1.6 %copy.15 = bf16[32,2048]{1,0:T(8,128)(2,1)} copy(bf16[32,2048]{1,0:T(8,128)(2,1)} %shard_map.133) | data formatting | bytes 262144
